TPU v7x, 32 devices: a whole 2x2x4 slice. The times are simulated.
32 devices in a mesh: sp: 4 (over z), tp: 4 (over y, x), dp: 2 (over core).
Axes of the slice: x: 2, y: 2, z: 4, core: 2. Of those that a mesh axis runs over, the one named last changes fastest.
Arguments:
- latent: bfloat16 [2, 1024, 2048], P('dp', 'sp'), may hold values from -1.5 to 1.5
- condition: bfloat16 [2, 2048], P('dp', 'sp'), may hold values from -6 to 6
- context: bfloat16 [2, 1024, 2048], P('dp', 'sp'), may hold values from -6 to 6
- context_code: bfloat16 [2048], P('sp'), may hold values from -6 to 6
- shift_weight: bfloat16 [2048, 2048], P('sp', 'tp'), may hold values from -0.125 to 0.125
- scale_weight: bfloat16 [2048, 2048], P('sp', 'tp'), may hold values from -0.125 to 0.125
- gate_weight: bfloat16 [2048, 2048], P('sp', 'tp'), may hold values from -0.125 to 0.125
- norm_gain: float32 [2048], replicated, may hold values from 0.1 to 1.9
- query_weight: bfloat16 [2048, 1024], P(None, 'tp'), may hold values from -0.125 to 0.125
- key_weight: bfloat16 [2048, 256], P(None, 'tp'), may hold values from -0.125 to 0.125
- value_weight: bfloat16 [2048, 256], P(None, 'tp'), may hold values from -0.125 to 0.125
- output_weight: bfloat16 [1024, 2048], P('tp'), may hold values from -0.75 to 0.75
- query_gain: float32 [64], replicated, may hold values from 1 to 5.5
- key_gain: float32 [64], replicated, may hold values from 1 to 5.5
- context_bias: float32 [16], P('tp'), may hold values from 0.5 to 2
Outputs:
- updated: bfloat16 [2, 1024, 2048], P('dp', 'sp')
All inputs are finite; a program needn't handle non-finite values.
Results may differ from a plain program's by a relative error of at most 0.01405.
The roundings to bfloat16 on the way count: a program that leaves them out, or rounds other values in their place, can miss the bound.
Values may be sent and summed in bfloat16 or wider, within the bound.
A program may use at most 64 MiB of HBM per device.

v0:
```python
import functools
import math

import jax
import jax.numpy as jnp
from jax import lax
from jax.experimental import pallas as pl
from jax.experimental.pallas import tpu as pltpu
from jax.sharding import PartitionSpec as P

GRID_W = 64
norm_eps = 1e-06
rope_base = 10000.0
F32 = jnp.float32
BF16 = jnp.bfloat16
LOW = -1e30


def tables(first, rows, head_dim):
    quarter = head_dim // 4
    half = head_dim // 2
    shape = (rows, head_dim)
    token = first + lax.broadcasted_iota(jnp.int32, shape, 0)
    lane = lax.broadcasted_iota(jnp.int32, shape, 1)
    pair = lane % half
    index = (pair % quarter).astype(F32)
    place = jnp.where(pair < quarter, token // GRID_W, token % GRID_W).astype(F32)
    angle = place * jnp.exp(index * (-math.log(rope_base) / quarter))
    sine = jnp.sin(angle)
    return jnp.cos(angle), jnp.where(lane < half, -sine, sine)


def head_norm(values, gain_row):
    mean = jnp.mean(values * values, axis=-1, keepdims=True)
    return values * lax.rsqrt(mean + norm_eps) * gain_row


def rotate(values, cosine, sine):
    half = values.shape[-1] // 2
    swapped = jnp.concatenate([values[:, half:], values[:, :half]], axis=1)
    return values * cosine + swapped * sine


def kernel(
    sizes,
    condition, code, gain_ref, q_gain, k_gain, bias_ref,
    latent, context, shift_w, scale_w, gate_w, wq, wk, wv, wo,
    out,
    modw, lat, ctx, wq_v, wkv, wbuf,
    vec_z, vec_t, normed, kvbuf, q_s, m_s, acc, att, mixed, cos_s, sin_s, inv_s, out_v,
    local, out_sem,
    z_send, z_recv, t_send, t_recv, kv_send, kv_recv,
    w_send, w_recv, f_send, f_recv, a_send, a_recv,
):
    n_sp, n_tp, n_dp = sizes
    sp, tp, dp = lax.axis_index("sp"), lax.axis_index("tp"), lax.axis_index("dp")
    rows, crows = lat.shape[0], ctx.shape[0]
    hd = wk.shape[0]
    qcols = wq_v.shape[1]
    heads = qcols // hd
    width = lat.shape[1]
    cols = width // n_tp
    dots = functools.partial(jnp.dot, preferred_element_type=F32)

    copies = {}
    for number, (name, src, dst) in enumerate((
        ("m0", shift_w, modw.at[0]), ("m1", scale_w, modw.at[1]), ("m2", gate_w, modw.at[2]),
        ("wk", wk, wkv.at[:hd]), ("wv", wv, wkv.at[hd:]), ("ctx", context.at[0], ctx), ("lat", latent.at[0], lat),
        ("wq", wq, wq_v), ("wo", wo, wbuf.at[tp]),
    )):
        copies[name] = pltpu.make_async_copy(src, dst, local.at[number])
        copies[name].start()

    barrier = pltpu.get_barrier_semaphore()
    for d in range(1, n_sp):
        pl.semaphore_signal(barrier, inc=1, device_id={"sp": (sp + d) % n_sp}, device_id_type=pl.DeviceIdType.MESH)
    for d in range(1, n_tp):
        pl.semaphore_signal(barrier, inc=1, device_id={"tp": tp ^ d}, device_id_type=pl.DeviceIdType.MESH)
    for d in range(1, n_dp):
        pl.semaphore_signal(barrier, inc=1, device_id={"dp": (dp + d) % n_dp}, device_id_type=pl.DeviceIdType.MESH)

    def remote(src, dst, s, r, **where):
        return pltpu.make_async_remote_copy(
            src_ref=src, dst_ref=dst, send_sem=s, recv_sem=r,
            device_id=where, device_id_type=pl.DeviceIdType.MESH)

    row8 = lax.broadcasted_iota(jnp.int32, (8, condition.shape[1]), 0)
    own_code = condition[...].astype(F32)
    shared_code = code[...].astype(F32)[None]
    both = jnp.where(row8 == 0, own_code, jnp.where(row8 == 1, shared_code, 0.0))
    both = (both / (1.0 + jnp.exp(-both))).astype(BF16)
    pieces = []
    for k in range(3):
        copies[f"m{k}"].wait()
        pieces.append(dots(both, modw[k])[:2])
    vec_z[sp] = jnp.concatenate(pieces + [jnp.zeros_like(pieces[0])], axis=0)

    pl.semaphore_wait(barrier, n_sp + n_tp + n_dp - 3)
    z_copies = []
    for d in range(1, n_sp):
        copy = remote(vec_z.at[sp], vec_z.at[sp], z_send.at[d], z_recv.at[d], sp=(sp + d) % n_sp)
        copy.start()
        z_copies.append(copy)

    share = wo.shape[0] // n_dp
    piece = share // 2

    def span(core, part):
        return pl.ds(core * share + part * piece, piece)

    near = [d for d in (1, 2) if d < n_tp]
    waiting = []

    def send_weights(part):
        for d in near:
            copy = remote(wo.at[span(dp, part)], wbuf.at[tp, span(dp, part)],
                          w_send.at[d, part], w_recv.at[d, part], tp=tp ^ d)
            copy.start()
            waiting.append(copy)

    def got_weights(d, part):
        ref = wbuf.at[tp ^ d, span(dp, part)]
        remote(ref, ref, w_send.at[d, part], w_recv.at[d, part], tp=tp ^ d).wait_recv()
        if n_tp == 4 and (d, part) in ((2, 0), (1, 1)):
            copy = remote(ref, ref, w_send.at[3, part], w_recv.at[3, part], tp=tp ^ (3 - d))
            copy.start()
            waiting.append(copy)
        for e in range(1, n_dp):
            copy = remote(ref, ref, f_send.at[d, part, e], f_recv.at[d, part, e], dp=(dp + e) % n_dp)
            copy.start()
            waiting.append(copy)

    send_weights(0)

    cosine, sine = tables(sp * rows, rows, hd)
    cos_s[...] = cosine
    sin_s[...] = sine
    copies["ctx"].wait()
    floats = ctx[...].astype(F32)
    inv_c = lax.rsqrt(jnp.mean(floats * floats, axis=-1, keepdims=True) + norm_eps)
    copies["lat"].wait()
    floats = lat[...].astype(F32)
    inv_s[...] = lax.rsqrt(jnp.mean(floats * floats, axis=-1, keepdims=True) + norm_eps)

    for copy in z_copies:
        copy.wait()
    total = vec_z[0]
    for k in range(1, n_sp):
        total = total + vec_z[k]
    vec_t[tp] = total
    for d in range(1, n_tp):
        copy = remote(vec_t.at[tp], vec_t.at[tp], t_send.at[d], t_recv.at[d], tp=tp ^ d)
        copy.start()
        waiting.append(copy)
    send_weights(1)
    for d in range(1, n_tp):
        remote(vec_t.at[tp ^ d], vec_t.at[tp ^ d], t_send.at[d], t_recv.at[d], tp=tp ^ d).wait_recv()

    def modulate(tokens, inverse, which):
        for t in range(n_tp):
            part = slice(t * cols, (t + 1) * cols)
            factor = gain_ref[:, part] * (1.0 + vec_t[t, 2 + which:3 + which, :])
            shift = vec_t[t, which:which + 1, :]
            normed[:tokens.shape[0], part] = (tokens[:, part].astype(F32) * inverse * factor + shift).astype(BF16)

    lanes = 2 * hd

    def kv_copy(block, target, way, part):
        area = pl.ds(0, crows) if part == 0 else pl.ds(crows, rows)
        ref = kvbuf.at[block, area]
        return remote(ref, ref, kv_send.at[way, part, block], kv_recv.at[part, block], sp=target)

    def send_own(part):
        @pl.when(sp + 1 < n_sp)
        def _():
            kv_copy(sp, sp + 1, 0, part).start()

        @pl.when(sp > 0)
        def _():
            kv_copy(sp, sp - 1, 1, part).start()

    dims = (((1,), (1,)), ((), ()))
    modulate(ctx, inv_c, 1)
    copies["wk"].wait()
    copies["wv"].wait()
    kv = lax.dot_general(normed[:crows], wkv[...], dims, preferred_element_type=F32)
    kvbuf[sp, :crows] = jnp.concatenate([head_norm(kv[:, :hd], k_gain[...]), kv[:, hd:]], axis=1).astype(BF16)
    send_own(0)

    modulate(lat, inv_s[...], 0)
    kv = lax.dot_general(normed[:rows], wkv[...], dims, preferred_element_type=F32)
    keys = rotate(head_norm(kv[:, :hd], k_gain[...]), cos_s[...], sin_s[...])
    kvbuf[sp, crows:] = jnp.concatenate([keys, kv[:, hd:]], axis=1).astype(BF16)
    send_own(1)

    copies["wq"].wait()
    queries = dots(normed[:rows], wq_v[...])
    for h in range(heads):
        one = rotate(head_norm(queries[:, h * hd:(h + 1) * hd], q_gain[...]), cos_s[...], sin_s[...])
        q_s[h] = (one * hd ** -0.5).astype(BF16)
    m_s[...] = jnp.full_like(m_s, LOW)
    acc[...] = jnp.zeros_like(acc)

    for d in near:
        got_weights(d, 0)

    def absorb(block):
        @pl.loop(0, heads, unroll=2)
        def _(h):
            bias = bias_ref[h]
            query = q_s[h]
            s_c = lax.dot_general(query, kvbuf[block, :crows, :hd], dims, preferred_element_type=F32)
            s_l = lax.dot_general(query, kvbuf[block, crows:, :hd], dims, preferred_element_type=F32)
            old = m_s[h]
            new = jnp.maximum(old, jnp.maximum(
                s_c.max(axis=1, keepdims=True) + bias, s_l.max(axis=1, keepdims=True)))
            m_s[h] = new
            p_c = jnp.exp(s_c - (new - bias)).astype(BF16)
            p_l = jnp.exp(s_l - new).astype(BF16)

            def values(pairs):
                lane = lax.broadcasted_iota(jnp.int32, pairs.shape, 1)
                return jnp.where(lane < hd, jnp.ones_like(pairs), pairs)

            acc[h] = (acc[h] * jnp.exp(old - new)
                      + dots(p_c, values(kvbuf[block, :crows]))
                      + dots(p_l, values(kvbuf[block, crows:])))

    absorb(sp)

    def forward(s):
        for part in range(2):
            @pl.when(sp - s >= 0)
            def _():
                kv_copy(sp - s, sp, 0, part).wait_recv()

                @pl.when(sp + 1 < n_sp)
                def _():
                    kv_copy(sp - s, sp + 1, 0, part).start()

            @pl.when(sp + s < n_sp)
            def _():
                kv_copy(sp + s, sp, 1, part).wait_recv()

                @pl.when(sp > 0)
                def _():
                    kv_copy(sp + s, sp - 1, 1, part).start()

    def absorb_both(s):
        @pl.when(sp - s >= 0)
        def _():
            absorb(sp - s)

        @pl.when(sp + s < n_sp)
        def _():
            absorb(sp + s)

    if n_sp > 1:
        forward(1)
    for d in near:
        got_weights(d, 1)
    if n_sp > 1:
        absorb_both(1)

    @pl.loop(2, n_sp)
    def _(s):
        forward(s)
        absorb_both(s)

    if n_tp == 4:
        for part in range(2):
            got_weights(3, part)

    for g in range(heads // 2):
        pair = []
        for h in (2 * g, 2 * g + 1):
            whole = acc[h]
            pair.append(whole[:, hd:] / whole[:, :hd])
        att[tp, g] = jnp.concatenate(pair, axis=1).astype(BF16)
        for d in range(1, n_tp):
            copy = remote(att.at[tp, g], att.at[tp, g], a_send.at[d, g], a_recv.at[d, g], tp=tp ^ d)
            copy.start()
            waiting.append(copy)

    copies["wo"].wait()
    step = cols

    def project(group):
        left = jnp.concatenate([att[group, g] for g in range(heads // 2)], axis=1)
        return lambda part: dots(left, wbuf[group, :, part]).astype(BF16).astype(F32)

    def arrive(d):
        for core in range(1, n_dp):
            source = (dp + n_dp - core) % n_dp
            for part in range(2):
                ref = wbuf.at[tp ^ d, span(source, part)]
                remote(ref, ref, f_send.at[d, part, core], f_recv.at[d, part, core], dp=source).wait_recv()
        for g in range(heads // 2):
            ref = att.at[tp ^ d, g]
            remote(ref, ref, a_send.at[d, g], a_recv.at[d, g], tp=tp ^ d).wait_recv()
        return project(tp ^ d)

    backs = []
    for d in range(n_tp):
        term = project(tp) if d == 0 else arrive(d)
        for t in range(n_tp):
            part = slice(t * step, (t + 1) * step)
            value = term(part)
            if d > 0:
                value = mixed[:, part] + value
            if d < n_tp - 1:
                mixed[:, part] = value
            else:
                gate = vec_t[t, 4:5, :]
                out_v[:, part] = (lat[:, part].astype(F32) + gate * value).astype(BF16)
                back = pltpu.make_async_copy(out_v.at[:, part], out.at[0, :, part], out_sem.at[t])
                back.start()
                backs.append(back)

    for copy in waiting:
        copy.wait_send()

    @pl.loop(0, n_sp)
    def _(b):
        for part in range(2):
            @pl.when((b <= sp) & (sp + 1 < n_sp))
            def _():
                kv_copy(b, sp, 0, part).wait_send()

            @pl.when((b >= sp) & (sp > 0))
            def _():
                kv_copy(b, sp, 1, part).wait_send()
    for back in backs:
        back.wait()


def on_device(
    sizes, latent, condition, context, context_code, shift_weight, scale_weight, gate_weight,
    norm_gain, query_weight, key_weight, value_weight, output_weight, query_gain, key_gain,
    context_bias,
):
    n_sp, n_tp, n_dp = sizes
    rows, width = latent.shape[1:]
    crows = context.shape[1]
    hd = query_gain.shape[0]
    qcols = query_weight.shape[1]
    heads = qcols // hd
    deep, cols = shift_weight.shape
    vmem = pl.BlockSpec(memory_space=pltpu.VMEM)
    smem = pl.BlockSpec(memory_space=pltpu.SMEM)
    hbm = pl.BlockSpec(memory_space=pl.ANY)
    dma = pltpu.SemaphoreType.DMA
    most = max(rows, crows)
    scratch = [
        pltpu.VMEM((3, deep, cols), BF16),
        pltpu.VMEM((rows, width), BF16),
        pltpu.VMEM((crows, width), BF16),
        pltpu.VMEM((width, qcols), BF16),
        pltpu.VMEM((2 * hd, width), BF16),
        pltpu.VMEM((n_tp,) + output_weight.shape, BF16),
        pltpu.VMEM((n_sp, 8, cols), F32),
        pltpu.VMEM((n_tp, 8, cols), F32),
        pltpu.VMEM((most, width), BF16),
        pltpu.VMEM((n_sp, crows + rows, 2 * hd), BF16),
        pltpu.VMEM((heads, rows, hd), BF16),
        pltpu.VMEM((heads, rows, 1), F32),
        pltpu.VMEM((heads, rows, 2 * hd), F32),
        pltpu.VMEM((n_tp, heads // 2, rows, 2 * hd), BF16),
        pltpu.VMEM((rows, width), F32),
        pltpu.VMEM((rows, hd), F32),
        pltpu.VMEM((rows, hd), F32),
        pltpu.VMEM((rows, 1), F32),
        pltpu.VMEM((rows, width), BF16),
        dma((9,)), dma((n_tp,)),
        dma((n_sp,)), dma((n_sp,)), dma((n_tp,)), dma((n_tp,)),
        dma((2, 2, n_sp)), dma((2, n_sp)),
        dma((n_tp, 2)), dma((n_tp, 2)), dma((n_tp, 2, n_dp)), dma((n_tp, 2, n_dp)),
        dma((n_tp, heads // 2)), dma((n_tp, heads // 2)),
    ]
    return pl.pallas_call(
        functools.partial(kernel, sizes),
        out_shape=jax.ShapeDtypeStruct(latent.shape, BF16),
        in_specs=[vmem] * 5 + [smem] + [hbm] * 9,
        out_specs=hbm,
        scratch_shapes=scratch,
        compiler_params=pltpu.CompilerParams(
            collective_id=0, has_side_effects=True, vmem_limit_bytes=60 * 1024 * 1024),
    )(
        condition, context_code, norm_gain[None], query_gain[None], key_gain[None],
        context_bias, latent, context, shift_weight, scale_weight, gate_weight, query_weight,
        key_weight.T, value_weight.T, output_weight,
    )


def solution(mesh):
    sizes = tuple(mesh.shape[axis] for axis in ("sp", "tp", "dp"))
    return jax.shard_map(
        functools.partial(on_device, sizes),
        mesh=mesh,
        in_specs=(
            P("dp", "sp", None),
            P("dp", "sp"),
            P("dp", "sp", None),
            P("sp"),
            P("sp", "tp"),
            P("sp", "tp"),
            P("sp", "tp"),
            P(),
            P(None, "tp"),
            P(None, "tp"),
            P(None, "tp"),
            P("tp", None),
            P(),
            P(),
            P("tp"),
        ),
        out_specs=P("dp", "sp", None),
        check_vma=False,
    )
```

profile of v0, /device:TPU:0, one launch (start us, length us, event | category | flops | bytes accessed | tf_op | source)
XLA Modules:
  0.0 41.9 jit_solution(8946033876914509770)
XLA Ops:
  0.0 39.6 %shard_map.145 = bf16[1,256,2048]{2,1,0:T(8,128)(2,1)} custom-call(bf16[1,512]{1,0:T(2,128)(2,1)} %condition.1, bf16[512]{0:T(512)(128)(2,1)} %code.1, f32[1,2048]{1,0:T(1,128)} %bitcast.7, f32[1,64]{1,0:T(1,128)} %bitcast.8, f32[1,64]{1,0:T(1,128)} %bitcast.9, f32[4]{0:T(128)} %bias_ref.1, bf16[1,256,2048]{2,1,0:T(8,128)(2,1)} %latent.1, ...), custom_call_target="tpu_custom_call" | custom-call | tf_op jit(solution)/shard_map/pallas_call | solution.py:380
  39.6 2.3 %copy.17 = bf16[1,256,2048]{2,1,0:T(8,128)(2,1)} copy(bf16[1,256,2048]{2,1,0:T(8,128)(2,1)} %shard_map.145) | data formatting | bytes 2097152
where the time goes:
time: 42.1 us; the launch traced here: 41.9 us
  Pallas kernels  39.6 us (94%)
  local copies, waits for them, and re-layouts  2.3 us (5%)
    pallas_call x1, Pallas kernels, on_device(): pl.pallas_call(functools.partial(kernel, sizes), out_shape=jax.ShapeDtype...  39.6 us
    unnamed x1, local copies, waits for them, and re-layouts  2.3 us

commit v1 on v0

v1 whole, which is shorter than its diff:
```python
import functools
import math

import jax
import jax.numpy as jnp
from jax import lax
from jax.experimental import pallas as pl
from jax.experimental.pallas import tpu as pltpu
from jax.sharding import PartitionSpec as P

GRID_W = 64
norm_eps = 1e-06
rope_base = 10000.0
F32 = jnp.float32
BF16 = jnp.bfloat16
LANES = 128
LOG2E = math.log2(math.e)
PARTS = 4
SCOPED_KIB = 64384


def tables(first, rows, head_dim):
    quarter = head_dim // 4
    half = head_dim // 2
    shape = (rows, 2 * head_dim)
    token = first + lax.broadcasted_iota(jnp.int32, shape, 0)
    lane = lax.broadcasted_iota(jnp.int32, shape, 1) % head_dim
    pair = lane % half
    index = (pair % quarter).astype(F32)
    place = jnp.where(pair < quarter, token // GRID_W, token % GRID_W).astype(F32)
    angle = place * jnp.exp(index * (-math.log(rope_base) / quarter))
    sine = jnp.sin(angle)
    return jnp.cos(angle), jnp.where(lane < half, -sine, sine)


def kernel(
    sizes,
    condition, code, gain_ref, q_gain, k_gain, bias_ref,
    latent, context, shift_w, scale_w, gate_w, wq, wk, wv, wo,
    out,
    modw, lat, ctx, wq_v, wkv, wbuf,
    vec_z, vec_t, gate_z, gate_t, normed, kvbuf, vals, q_s, m_s, acc, att, mixed, cos_s, sin_s, inv_s,
    local, met,
    z_send, z_recv, t_send, t_recv, gz_send, gz_recv, gt_send, gt_recv, kv_send, kv_recv,
    w_send, w_recv, f_send, f_recv, a_send, a_recv,
):
    n_sp, n_tp, n_dp = sizes
    sp, tp, dp = lax.axis_index("sp"), lax.axis_index("tp"), lax.axis_index("dp")
    rows, crows = lat.shape[0], ctx.shape[0]
    hd = wk.shape[0]
    qcols = wq_v.shape[1]
    heads = qcols // hd
    width = lat.shape[1]
    cols = width // n_tp
    side = cols // 2
    chip = cols // 4
    mid = rows // 2
    lanes = 2 * hd
    dots = functools.partial(jnp.dot, preferred_element_type=F32)
    dims = (((1,), (1,)), ((), ()))
    scope = jax.named_scope

    copies = {}
    for number, (name, src, dst) in enumerate((
        ("m0", shift_w, modw.at[0]), ("m1", scale_w, modw.at[1]),
        ("ctx", context.at[0], ctx), ("wk", wk, wkv.at[:hd]), ("wv", wv, wkv.at[hd:]),
        ("m2", gate_w, modw.at[2]), ("lat", latent.at[0], lat),
        ("wq", wq, wq_v), ("wo", wo, wbuf.at[tp]),
    )):
        copies[name] = pltpu.make_async_copy(src, dst, local.at[number])
        copies[name].start()

    barrier = pltpu.get_barrier_semaphore()

    def greet(sem, **where):
        pl.semaphore_signal(sem, inc=1, device_id=where, device_id_type=pl.DeviceIdType.MESH)

    for d in range(1, n_sp):
        greet(barrier, sp=(sp + d) % n_sp)
    for d in range(1, n_tp):
        greet(barrier, tp=tp ^ d)
    for d in range(1, n_dp):
        @pl.when(dp + d < n_dp)
        def _():
            greet(barrier, dp=dp + d)

    def remote(src, dst, s, r, **where):
        return pltpu.make_async_remote_copy(
            src_ref=src, dst_ref=dst, send_sem=s, recv_sem=r,
            device_id=where, device_id_type=pl.DeviceIdType.MESH)

    with scope("modmat"):
        row8 = lax.broadcasted_iota(jnp.int32, (8, condition.shape[1]), 0)
        own_code = condition[...].astype(F32)
        shared_code = code[...].astype(F32)[None]
        both = jnp.where(row8 == 0, own_code, jnp.where(row8 == 1, shared_code, 0.0))
        both = (both / (1.0 + jnp.exp(-both))).astype(BF16)
        pieces = []
        for k in range(2):
            copies[f"m{k}"].wait()
            pieces.append(dots(both, modw[k])[:2])
        rows4 = jnp.concatenate(pieces, axis=0)
        vec_z[sp] = jnp.concatenate([rows4[:, :side], rows4[:, side:]], axis=0)

    with scope("barrier"):
        pl.semaphore_wait(barrier, n_sp + n_tp - 2 + dp)

    z_copies = []
    for d in range(1, n_sp):
        copy = remote(vec_z.at[sp], vec_z.at[sp], z_send.at[d], z_recv.at[d], sp=(sp + d) % n_sp)
        copy.start()
        z_copies.append(copy)
    for d in range(1, n_dp):
        @pl.when(dp - d >= 0)
        def _():
            greet(met, dp=dp - d)

    share = wo.shape[0] // n_dp
    piece = share // PARTS
    near = [d for d in (1, 2) if d < n_tp]
    turns = {1: (2, 3, 0, 1), 2: (0, 1, 2, 3)}
    waiting = []

    def span(core, part):
        return pl.ds(core * share + part * piece, piece)

    def send_weights(turn):
        for d in near:
            part = turns[d][turn]
            copy = remote(wo.at[span(dp, part)], wbuf.at[tp, span(dp, part)],
                          w_send.at[d, part], w_recv.at[d, part], tp=tp ^ d)
            copy.start()
            waiting.append(copy)

    def got_weights(d, part):
        ref = wbuf.at[tp ^ d, span(dp, part)]
        remote(ref, ref, w_send.at[d, part], w_recv.at[d, part], tp=tp ^ d).wait_recv()
        if n_tp == 4 and d < 3 and part in turns[d][:2]:
            copy = remote(ref, ref, w_send.at[3, part], w_recv.at[3, part], tp=tp ^ (3 - d))
            copy.start()
            waiting.append(copy)
        for e in range(1, n_dp):
            copy = remote(ref, ref, f_send.at[d, part, e], f_recv.at[d, part, e], dp=(dp + e) % n_dp)
            copy.start()
            waiting.append(copy)

    send_weights(0)

    with scope("gate"):
        copies["m2"].wait()
        row = dots(both, modw[2])[:1]
        gate_z[sp] = jnp.concatenate([row[:, j * chip:(j + 1) * chip] for j in range(4)], axis=0)
    g_copies = []
    for d in range(1, n_sp):
        copy = remote(gate_z.at[sp], gate_z.at[sp], gz_send.at[d], gz_recv.at[d], sp=(sp + d) % n_sp)
        copy.start()
        g_copies.append(copy)

    with scope("tables"):
        cosine, sine = tables(sp * rows, rows, hd)
        cos_s[...] = cosine
        sin_s[...] = sine
    with scope("inv"):
        copies["ctx"].wait()
        floats = ctx[...].astype(F32)
        inv_c = lax.rsqrt(jnp.mean(floats * floats, axis=-1, keepdims=True) + norm_eps)
        copies["lat"].wait()
        floats = lat[...].astype(F32)
        inv_s[...] = lax.rsqrt(jnp.mean(floats * floats, axis=-1, keepdims=True) + norm_eps)

    with scope("zwait"):
        for copy in z_copies:
            copy.wait()
    total = vec_z[0]
    for k in range(1, n_sp):
        total = total + vec_z[k]
    vec_t[tp] = total
    for d in reversed(range(1, n_tp)):
        copy = remote(vec_t.at[tp], vec_t.at[tp], t_send.at[d], t_recv.at[d], tp=tp ^ d)
        copy.start()
        waiting.append(copy)
    for turn in range(1, PARTS):
        send_weights(turn)
    with scope("twait"):
        for d in range(1, n_tp):
            remote(vec_t.at[tp ^ d], vec_t.at[tp ^ d], t_send.at[d], t_recv.at[d], tp=tp ^ d).wait_recv()

    def modulate(tokens, inverse, which):
        for t in range(n_tp):
            for k in range(2):
                part = slice(t * cols + k * side, t * cols + (k + 1) * side)
                at = 4 * k + which
                factor = gain_ref[:, part] * (1.0 + vec_t[t, at + 2:at + 3, :])
                shift = vec_t[t, at:at + 1, :]
                normed[:tokens.shape[0], part] = (tokens[:, part].astype(F32) * inverse * factor + shift).astype(BF16)

    def kv_copy(block, target, way, part):
        area = pl.ds(0, crows) if part == 0 else pl.ds(crows, rows)
        ref = kvbuf.at[block, area]
        return remote(ref, ref, kv_send.at[way, part, block], kv_recv.at[part, block], sp=target)

    def send_own(part):
        @pl.when(sp + 1 < n_sp)
        def _():
            kv_copy(sp, sp + 1, 0, part).start()

        @pl.when(sp > 0)
        def _():
            kv_copy(sp, sp - 1, 1, part).start()

    def averages(values):
        n = values.shape[1]
        row = lax.broadcasted_iota(jnp.int32, (n, n), 0) // hd
        col = lax.broadcasted_iota(jnp.int32, (n, n), 1) // hd
        spread = jnp.where(row == col, 1.0 / hd, 0.0).astype(BF16)
        return dots((values * values).astype(BF16), spread)

    def swapped(values):
        lane = lax.broadcasted_iota(jnp.int32, values.shape, 1) % hd
        return jnp.where(lane < hd // 2, pltpu.roll(values, lanes - hd // 2, 1), pltpu.roll(values, hd // 2, 1))

    def key_values(count, turn):
        kv = lax.dot_general(normed[:count], wkv[...], dims, preferred_element_type=F32)
        lane = lax.broadcasted_iota(jnp.int32, kv.shape, 1)
        keys = kv * lax.rsqrt(averages(kv) + norm_eps) * jnp.concatenate([k_gain[...]] * 2, axis=1)
        if turn:
            keys = keys * cos_s[...] + swapped(keys) * sin_s[...]
        return jnp.where(lane < hd, keys, kv).astype(BF16)

    with scope("modctx"):
        modulate(ctx, inv_c, 1)
    with scope("kvctx"):
        copies["wk"].wait()
        copies["wv"].wait()
        kvbuf[sp, :crows] = key_values(crows, False)
    send_own(0)

    with scope("modlat"):
        modulate(lat, inv_s[...], 0)
    with scope("kvlat"):
        kvbuf[sp, crows:] = key_values(rows, True)
    send_own(1)

    with scope("gotw0"):
        for d in range(1, n_dp):
            @pl.when(dp + d < n_dp)
            def _():
                pl.semaphore_wait(met, 1)
        for d in near:
            got_weights(d, turns[d][0])

    with scope("qproj"):
        copies["wq"].wait()
        queries = dots(normed[:rows], wq_v[...])
        factor = lax.rsqrt(averages(queries) + norm_eps)
        gains = jnp.concatenate([q_gain[...]] * 2, axis=1) * (hd ** -0.5 * LOG2E)
        lane = lax.broadcasted_iota(jnp.int32, (rows, lanes), 1)
        for g in range(heads // 2):
            pair = slice(g * lanes, (g + 1) * lanes)
            two = queries[:, pair] * factor[:, pair] * gains
            two = two * cos_s[...] + swapped(two) * sin_s[...]
            for h, one in ((2 * g, two), (2 * g + 1, pltpu.roll(two, hd, 1))):
                one = jnp.where(lane < hd, one, 0.0).astype(BF16)
                for half in range(2):
                    q_s[half, h * mid:(h + 1) * mid] = one[half * mid:(half + 1) * mid]

    with scope("gatez"):
        for copy in g_copies:
            copy.wait()
        total = gate_z[0]
        for k in range(1, n_sp):
            total = total + gate_z[k]
        gate_t[tp] = total
    for d in range(1, n_tp):
        copy = remote(gate_t.at[tp], gate_t.at[tp], gt_send.at[d], gt_recv.at[d], tp=tp ^ d)
        copy.start()
        waiting.append(copy)

    def spread(column, count):
        if count % LANES == 0:
            return jnp.concatenate([column] * (count // LANES), axis=1)
        return column[:, :count]

    def prepare(block):
        pairs = kvbuf[block]
        lane = lax.broadcasted_iota(jnp.int32, pairs.shape, 1)
        vals[...] = jnp.where(lane < hd, jnp.ones_like(pairs), pairs)

    def absorb(block, half, first=False):
        def scores(h):
            query = q_s[half, h * mid:(h + 1) * mid]
            return (lax.dot_general(query, kvbuf[block, :crows], dims, preferred_element_type=F32),
                    lax.dot_general(query, kvbuf[block, crows:], dims, preferred_element_type=F32))

        ahead = scores(0)
        for h in range(heads):
            s_c, s_l = ahead
            if h + 1 < heads:
                ahead = scores(h + 1)
            bias = bias_ref[h] * LOG2E
            top = jnp.maximum(s_c.max(axis=1, keepdims=True) + bias, s_l.max(axis=1, keepdims=True))
            top = jnp.broadcast_to(top, (mid, lanes))
            new = top if first else jnp.maximum(m_s[half, h], top)
            p_c = jnp.exp2(s_c - spread(new - bias, crows)).astype(BF16)
            p_l = jnp.exp2(s_l - spread(new, rows)).astype(BF16)
            more = dots(p_c, vals[:crows]) + dots(p_l, vals[crows:])
            if first:
                acc[half, h] = more
            else:
                acc[half, h] = acc[half, h] * jnp.exp2(m_s[half, h] - new) + more
            m_s[half, h] = new

    def absorb_all(block, first=False):
        prepare(block)

        @pl.loop(0, 2)
        def _(half):
            absorb(block, half, first)

    with scope("absorb0"):
        absorb_all(sp, True)

    with scope("gotw1"):
        for d in near:
            got_weights(d, turns[d][1])

    last = jnp.where(2 * sp < n_sp, n_sp - 1, 0)

    def forward(s):
        for part in range(2):
            @pl.when(sp - s >= 0)
            def _():
                kv_copy(sp - s, sp, 0, part).wait_recv()

                @pl.when(sp + 1 < n_sp)
                def _():
                    kv_copy(sp - s, sp + 1, 0, part).start()

            @pl.when(sp + s < n_sp)
            def _():
                kv_copy(sp + s, sp, 1, part).wait_recv()

                @pl.when(sp > 0)
                def _():
                    kv_copy(sp + s, sp - 1, 1, part).start()

    @pl.loop(1, n_sp)
    def _(s):
        with scope("fwd"):
            forward(s)

        @pl.loop(0, 2)
        def _(way):
            block = sp + s * (2 * way - 1)

            @pl.when((block >= 0) & (block < n_sp) & (block != last))
            def _():
                with scope("absorb"):
                    absorb_all(block)

    if n_sp > 1:
        with scope("prepare"):
            prepare(last)
    lane = lax.broadcasted_iota(jnp.int32, (mid, lanes), 1)
    for half in range(2):
        if n_sp > 1:
            with scope("final"):
                absorb(last, half)
        for g in range(heads // 2):
            even, odd = acc[half, 2 * g], acc[half, 2 * g + 1]
            top = jnp.where(lane < hd, pltpu.roll(even, hd, 1), odd)
            low = jnp.where(lane < hd, even, pltpu.roll(odd, hd, 1))
            att[tp, half, :, g * lanes:(g + 1) * lanes] = (top / low).astype(BF16)
        for d in reversed(range(1, n_tp)):
            copy = remote(att.at[tp, half], att.at[tp, half], a_send.at[d, half], a_recv.at[d, half], tp=tp ^ d)
            copy.start()
            waiting.append(copy)

    with scope("gotw2"):
        for d in near:
            for part in turns[d][2:]:
                got_weights(d, part)
    copies["wo"].wait()

    def project(group, half, part):
        return dots(att[group, half], wbuf[group, :, part])

    parts = [slice(t * cols, (t + 1) * cols) for t in range(n_tp)]
    tall = [slice(half * mid, (half + 1) * mid) for half in range(2)]
    with scope("own"):
        for half in range(2):
            for part in parts:
                mixed[tall[half], part] = project(tp, half, part)

    with scope("gotw3"):
        if n_tp == 4:
            for part in range(PARTS):
                got_weights(3, part)
        for d in range(1, n_tp):
            for core in range(1, n_dp):
                source = (dp + n_dp - core) % n_dp
                for part in range(PARTS):
                    ref = wbuf.at[tp ^ d, span(source, part)]
                    remote(ref, ref, f_send.at[d, part, core], f_recv.at[d, part, core], dp=source).wait_recv()
            remote(gate_t.at[tp ^ d], gate_t.at[tp ^ d], gt_send.at[d], gt_recv.at[d], tp=tp ^ d).wait_recv()

    order = [d for d in (2, 3, 1) if d < n_tp]
    for half in range(2):
        for d in order:
            with scope(f"att{half}{d}"):
                ref = att.at[tp ^ d, half]
                remote(ref, ref, a_send.at[d, half], a_recv.at[d, half], tp=tp ^ d).wait_recv()
            if d != order[-1]:
                for part in parts:
                    mixed[tall[half], part] = mixed[tall[half], part] + project(tp ^ d, half, part)
        for t, part in enumerate(parts):
            value = mixed[tall[half], part]
            if order:
                value = value + project(tp ^ order[-1], half, part)
            gate = jnp.concatenate([gate_t[t, j:j + 1, :] for j in range(4)], axis=1)
            out[0, tall[half], part] = (lat[tall[half], part].astype(F32) + gate * value).astype(BF16)

    with scope("sendwait"):
        for copy in waiting:
            copy.wait_send()

        @pl.loop(0, n_sp)
        def _(b):
            for part in range(2):
                @pl.when((b <= sp) & (sp + 1 < n_sp))
                def _():
                    kv_copy(b, sp, 0, part).wait_send()

                @pl.when((b >= sp) & (sp > 0))
                def _():
                    kv_copy(b, sp, 1, part).wait_send()


def on_device(
    sizes, latent, condition, context, context_code, shift_weight, scale_weight, gate_weight,
    norm_gain, query_weight, key_weight, value_weight, output_weight, query_gain, key_gain,
    context_bias,
):
    n_sp, n_tp, n_dp = sizes
    rows, width = latent.shape[1:]
    crows = context.shape[1]
    hd = query_gain.shape[0]
    qcols = query_weight.shape[1]
    heads = qcols // hd
    deep, cols = shift_weight.shape
    vmem = pl.BlockSpec(memory_space=pltpu.VMEM)
    smem = pl.BlockSpec(memory_space=pltpu.SMEM)
    hbm = pl.BlockSpec(memory_space=pl.ANY)
    dma = pltpu.SemaphoreType.DMA
    most = max(rows, crows)
    mid = rows // 2
    lanes = 2 * hd
    scratch = [
        pltpu.VMEM((3, deep, cols), BF16),
        pltpu.VMEM((rows, width), BF16),
        pltpu.VMEM((crows, width), BF16),
        pltpu.VMEM((width, qcols), BF16),
        pltpu.VMEM((lanes, width), BF16),
        pltpu.VMEM((n_tp,) + output_weight.shape, BF16),
        pltpu.VMEM((n_sp, 8, cols // 2), F32),
        pltpu.VMEM((n_tp, 8, cols // 2), F32),
        pltpu.VMEM((n_sp, 4, cols // 4), F32),
        pltpu.VMEM((n_tp, 4, cols // 4), F32),
        pltpu.VMEM((most, width), BF16),
        pltpu.VMEM((n_sp, crows + rows, lanes), BF16),
        pltpu.VMEM((crows + rows, lanes), BF16),
        pltpu.VMEM((2, heads * mid, lanes), BF16),
        pltpu.VMEM((2, heads, mid, lanes), F32),
        pltpu.VMEM((2, heads, mid, lanes), F32),
        pltpu.VMEM((n_tp, 2, mid, qcols), BF16),
        pltpu.VMEM((rows, width), F32),
        pltpu.VMEM((rows, lanes), F32),
        pltpu.VMEM((rows, lanes), F32),
        pltpu.VMEM((rows, 1), F32),
        dma((9,)), pltpu.SemaphoreType.REGULAR,
        dma((n_sp,)), dma((n_sp,)), dma((n_tp,)), dma((n_tp,)),
        dma((n_sp,)), dma((n_sp,)), dma((n_tp,)), dma((n_tp,)),
        dma((2, 2, n_sp)), dma((2, n_sp)),
        dma((n_tp, PARTS)), dma((n_tp, PARTS)), dma((n_tp, PARTS, n_dp)), dma((n_tp, PARTS, n_dp)),
        dma((n_tp, 2)), dma((n_tp, 2)),
    ]
    return pl.pallas_call(
        functools.partial(kernel, sizes),
        out_shape=pltpu.VMEM(latent.shape, BF16),
        in_specs=[vmem] * 5 + [smem] + [hbm] * 9,
        out_specs=vmem,
        scratch_shapes=scratch,
        compiler_params=pltpu.CompilerParams(
            collective_id=0, has_side_effects=True, vmem_limit_bytes=SCOPED_KIB * 1024),
    )(
        condition, context_code, norm_gain[None], query_gain[None], key_gain[None],
        context_bias, latent, context, shift_weight, scale_weight, gate_weight, query_weight,
        key_weight.T, value_weight.T, output_weight,
    )


def solution(mesh):
    sizes = tuple(mesh.shape[axis] for axis in ("sp", "tp", "dp"))
    return jax.shard_map(
        functools.partial(on_device, sizes),
        mesh=mesh,
        in_specs=(
            P("dp", "sp", None),
            P("dp", "sp"),
            P("dp", "sp", None),
            P("sp"),
            P("sp", "tp"),
            P("sp", "tp"),
            P("sp", "tp"),
            P(),
            P(None, "tp"),
            P(None, "tp"),
            P(None, "tp"),
            P("tp", None),
            P(),
            P(),
            P("tp"),
        ),
        out_specs=P("dp", "sp", None),
        check_vma=False,
    )
```

time: 42.1 us -> 35.7 us (0.85)
  Pallas kernels: 39.6 us -> 34.5 us
  local copies, waits for them, and re-layouts: 2.3 us -> 0.97 us
    pallas_call x1, Pallas kernels: 39.6 us -> 34.5 us  [on_device(): pl.pallas_call(functools.partial(kernel, sizes), out_shape=pltpu.VMEM(lat...]
    unnamed x1, local copies, waits for them, and re-layouts: 2.3 us -> 0.97 us
where the time goes in v1:
time: 35.7 us; the launch traced here: 35.5 us
  Pallas kernels  34.5 us (97%)
  local copies, waits for them, and re-layouts  0.97 us (3%)
    pallas_call x1, Pallas kernels, on_device(): pl.pallas_call(functools.partial(kernel, sizes), out_shape=pltpu.VMEM(lat...  34.5 us
    unnamed x1, local copies, waits for them, and re-layouts  0.97 us

profile of v1, /device:TPU:0, one launch (start us, length us, event | category | flops | bytes accessed | tf_op | source)
XLA Modules:
  0.0 35.5 jit_solution(8494759309611554098)
XLA Ops:
  0.0 34.5 %shard_map.145 = bf16[1,256,2048]{2,1,0:T(8,128)(2,1)S(1)} custom-call(bf16[1,512]{1,0:T(2,128)(2,1)} %condition.1, bf16[512]{0:T(512)(128)(2,1)} %code.1, f32[1,2048]{1,0:T(1,128)} %bitcast.7, f32[1,64]{1,0:T(1,128)} %bitcast.8, f32[1,64]{1,0:T(1,128)} %bitcast.9, f32[4]{0:T(128)} %bias_ref.1, bf16[1,256,2048]{2,1,0:T(8,128)(2,1)} %latent.1, ...), custom_call_target="tpu_custom_call" | custom-call | tf_op jit(solution)/shard_map/pallas_call | solution.py:487
  34.5 1.0 %copy.17 = bf16[1,256,2048]{2,1,0:T(8,128)(2,1)} copy(bf16[1,256,2048]{2,1,0:T(8,128)(2,1)S(1)} %shard_map.145) | data formatting | bytes 2097152

commit v2 on v1

--- a/solution.py
+++ b/solution.py
@@ -16,6 +16,7 @@
 LANES = 128
 LOG2E = math.log2(math.e)
 PARTS = 4
+GROUP = 2
 SCOPED_KIB = 64384
 
 
@@ -35,10 +36,11 @@
 
 def kernel(
     sizes,
-    condition, code, gain_ref, q_gain, k_gain, bias_ref,
+    condition_h, code_h, gain_h, q_gain_h, k_gain_h, bias_h,
     latent, context, shift_w, scale_w, gate_w, wq, wk, wv, wo,
     out,
-    modw, lat, ctx, wq_v, wkv, wbuf,
+    condition, code, gain_ref, q_gain, k_gain, bias_ref,
+    modw, lat, ctx, wq_v, wkv, wkv_t, wbuf,
     vec_z, vec_t, gate_z, gate_t, normed, kvbuf, vals, q_s, m_s, acc, att, mixed, cos_s, sin_s, inv_s,
     local, met,
     z_send, z_recv, t_send, t_recv, gz_send, gz_recv, gt_send, gt_recv, kv_send, kv_recv,
@@ -60,16 +62,6 @@
     dims = (((1,), (1,)), ((), ()))
     scope = jax.named_scope
 
-    copies = {}
-    for number, (name, src, dst) in enumerate((
-        ("m0", shift_w, modw.at[0]), ("m1", scale_w, modw.at[1]),
-        ("ctx", context.at[0], ctx), ("wk", wk, wkv.at[:hd]), ("wv", wv, wkv.at[hd:]),
-        ("m2", gate_w, modw.at[2]), ("lat", latent.at[0], lat),
-        ("wq", wq, wq_v), ("wo", wo, wbuf.at[tp]),
-    )):
-        copies[name] = pltpu.make_async_copy(src, dst, local.at[number])
-        copies[name].start()
-
     barrier = pltpu.get_barrier_semaphore()
 
     def greet(sem, **where):
@@ -84,12 +76,25 @@
         def _():
             greet(barrier, dp=dp + d)
 
+    copies = {}
+    for number, (name, src, dst) in enumerate((
+        ("condition", condition_h, condition), ("code", code_h, code),
+        ("m0", shift_w, modw.at[0]), ("m1", scale_w, modw.at[1]), ("m2", gate_w, modw.at[2]),
+        ("ctx", context.at[0], ctx), ("gain", gain_h, gain_ref), ("wk", wk, wkv.at[:hd]), ("wv", wv, wkv.at[hd:]),
+        ("k_gain", k_gain_h, k_gain), ("lat", latent.at[0], lat), ("q_gain", q_gain_h, q_gain), ("bias", bias_h, bias_ref),
+        ("wq", wq, wq_v), ("wo", wo, wbuf.at[tp]),
+    )):
+        copies[name] = pltpu.make_async_copy(src, dst, local.at[number])
+        copies[name].start()
+
     def remote(src, dst, s, r, **where):
         return pltpu.make_async_remote_copy(
             src_ref=src, dst_ref=dst, send_sem=s, recv_sem=r,
             device_id=where, device_id_type=pl.DeviceIdType.MESH)
 
     with scope("modmat"):
+        copies["condition"].wait()
+        copies["code"].wait()
         row8 = lax.broadcasted_iota(jnp.int32, (8, condition.shape[1]), 0)
         own_code = condition[...].astype(F32)
         shared_code = code[...].astype(F32)[None]
@@ -168,6 +173,10 @@
         floats = lat[...].astype(F32)
         inv_s[...] = lax.rsqrt(jnp.mean(floats * floats, axis=-1, keepdims=True) + norm_eps)
 
+    with scope("turn"):
+        copies["wk"].wait()
+        copies["wv"].wait()
+        wkv_t[...] = wkv[...].T
     with scope("zwait"):
         for copy in z_copies:
             copy.wait()
@@ -208,6 +217,16 @@
         def _():
             kv_copy(sp, sp - 1, 1, part).start()
 
+    def send_far(part):
+        if n_sp > 2:
+            @pl.when(sp == 0)
+            def _():
+                kv_copy(sp, n_sp - 1, 1, part).start()
+
+            @pl.when(sp == n_sp - 1)
+            def _():
+                kv_copy(sp, 0, 0, part).start()
+
     def averages(values):
         n = values.shape[1]
         row = lax.broadcasted_iota(jnp.int32, (n, n), 0) // hd
@@ -220,25 +239,27 @@
         return jnp.where(lane < hd // 2, pltpu.roll(values, lanes - hd // 2, 1), pltpu.roll(values, hd // 2, 1))
 
     def key_values(count, turn):
-        kv = lax.dot_general(normed[:count], wkv[...], dims, preferred_element_type=F32)
+        kv = dots(normed[:count], wkv_t[...])
         lane = lax.broadcasted_iota(jnp.int32, kv.shape, 1)
         keys = kv * lax.rsqrt(averages(kv) + norm_eps) * jnp.concatenate([k_gain[...]] * 2, axis=1)
         if turn:
             keys = keys * cos_s[...] + swapped(keys) * sin_s[...]
         return jnp.where(lane < hd, keys, kv).astype(BF16)
 
+    copies["gain"].wait()
     with scope("modctx"):
         modulate(ctx, inv_c, 1)
     with scope("kvctx"):
-        copies["wk"].wait()
-        copies["wv"].wait()
+        copies["k_gain"].wait()
         kvbuf[sp, :crows] = key_values(crows, False)
+    send_far(0)
     send_own(0)
 
     with scope("modlat"):
         modulate(lat, inv_s[...], 0)
     with scope("kvlat"):
         kvbuf[sp, crows:] = key_values(rows, True)
+    send_far(1)
     send_own(1)
 
     with scope("gotw0"):
@@ -251,6 +272,7 @@
 
     with scope("qproj"):
         copies["wq"].wait()
+        copies["q_gain"].wait()
         queries = dots(normed[:rows], wq_v[...])
         factor = lax.rsqrt(averages(queries) + norm_eps)
         gains = jnp.concatenate([q_gain[...]] * 2, axis=1) * (hd ** -0.5 * LOG2E)
@@ -287,28 +309,34 @@
         vals[...] = jnp.where(lane < hd, jnp.ones_like(pairs), pairs)
 
     def absorb(block, half, first=False):
-        def scores(h):
-            query = q_s[half, h * mid:(h + 1) * mid]
+        def scores(g):
+            query = q_s[half, g * GROUP * mid:(g + 1) * GROUP * mid]
             return (lax.dot_general(query, kvbuf[block, :crows], dims, preferred_element_type=F32),
                     lax.dot_general(query, kvbuf[block, crows:], dims, preferred_element_type=F32))
 
         ahead = scores(0)
-        for h in range(heads):
-            s_c, s_l = ahead
-            if h + 1 < heads:
-                ahead = scores(h + 1)
-            bias = bias_ref[h] * LOG2E
-            top = jnp.maximum(s_c.max(axis=1, keepdims=True) + bias, s_l.max(axis=1, keepdims=True))
-            top = jnp.broadcast_to(top, (mid, lanes))
-            new = top if first else jnp.maximum(m_s[half, h], top)
-            p_c = jnp.exp2(s_c - spread(new - bias, crows)).astype(BF16)
-            p_l = jnp.exp2(s_l - spread(new, rows)).astype(BF16)
-            more = dots(p_c, vals[:crows]) + dots(p_l, vals[crows:])
-            if first:
-                acc[half, h] = more
-            else:
-                acc[half, h] = acc[half, h] * jnp.exp2(m_s[half, h] - new) + more
-            m_s[half, h] = new
+        for g in range(heads // GROUP):
+            all_c, all_l = ahead
+            if (g + 1) * GROUP < heads:
+                ahead = scores(g + 1)
+            shares, weights_c, weights_l = [], [], []
+            for k in range(GROUP):
+                h = g * GROUP + k
+                s_c, s_l = all_c[k * mid:(k + 1) * mid], all_l[k * mid:(k + 1) * mid]
+                bias = bias_ref[h] * LOG2E
+                top = jnp.maximum(s_c.max(axis=1, keepdims=True) + bias, s_l.max(axis=1, keepdims=True))
+                top = jnp.broadcast_to(top, (mid, lanes))
+                new = top if first else jnp.maximum(m_s[half, h], top)
+                weights_c.append(jnp.exp2(s_c - spread(new - bias, crows)).astype(BF16))
+                weights_l.append(jnp.exp2(s_l - spread(new, rows)).astype(BF16))
+                shares.append(None if first else jnp.exp2(m_s[half, h] - new))
+                m_s[half, h] = new
+            more = (dots(jnp.concatenate(weights_c, axis=0), vals[:crows])
+                    + dots(jnp.concatenate(weights_l, axis=0), vals[crows:]))
+            for k in range(GROUP):
+                h = g * GROUP + k
+                own = more[k * mid:(k + 1) * mid]
+                acc[half, h] = own if first else acc[half, h] * shares[k] + own
 
     def absorb_all(block, first=False):
         prepare(block)
@@ -317,46 +345,75 @@
         def _(half):
             absorb(block, half, first)
 
+    lower = 2 * sp < n_sp
+    edge = (sp == 0) | (sp == n_sp - 1)
+
+    def away(s):
+        if n_sp < 3:
+            return s
+        return jnp.where(edge & (s > 1), jnp.where(s == 2, n_sp - 1, s - 1), s)
+
+    reach = jnp.where(edge, away(n_sp - 1), jnp.where(lower, n_sp - 1 - sp, sp))
+    last = jnp.where(lower, sp + reach, sp - reach)
+
+    def passes(block, target):
+        if n_sp < 3:
+            return (target >= 0) & (target < n_sp)
+        far = ((block == 0) & (target == n_sp - 1)) | ((block == n_sp - 1) & (target == 0))
+        return (target >= 0) & (target < n_sp) & jnp.logical_not(far)
+
+    def forward(s, parts=(0, 1)):
+        d = away(s)
+        for part in parts:
+            @pl.when(sp - d >= 0)
+            def _():
+                kv_copy(sp - d, sp, 0, part).wait_recv()
+
+                @pl.when(passes(sp - d, sp + 1))
+                def _():
+                    kv_copy(sp - d, sp + 1, 0, part).start()
+
+            @pl.when(sp + d < n_sp)
+            def _():
+                kv_copy(sp + d, sp, 1, part).wait_recv()
+
+                @pl.when(passes(sp + d, sp - 1))
+                def _():
+                    kv_copy(sp + d, sp - 1, 1, part).start()
+
+    copies["bias"].wait()
     with scope("absorb0"):
-        absorb_all(sp, True)
-
+        prepare(sp)
+        absorb(sp, 0, True)
+    if n_sp > 1:
+        with scope("fwd1c"):
+            forward(1, (0,))
+    with scope("absorb0"):
+        absorb(sp, 1, True)
+    if n_sp > 1:
+        with scope("fwd1l"):
+            forward(1, (1,))
     with scope("gotw1"):
         for d in near:
             got_weights(d, turns[d][1])
 
-    last = jnp.where(2 * sp < n_sp, n_sp - 1, 0)
-
-    def forward(s):
-        for part in range(2):
-            @pl.when(sp - s >= 0)
-            def _():
-                kv_copy(sp - s, sp, 0, part).wait_recv()
-
-                @pl.when(sp + 1 < n_sp)
-                def _():
-                    kv_copy(sp - s, sp + 1, 0, part).start()
-
-            @pl.when(sp + s < n_sp)
-            def _():
-                kv_copy(sp + s, sp, 1, part).wait_recv()
-
-                @pl.when(sp > 0)
-                def _():
-                    kv_copy(sp + s, sp - 1, 1, part).start()
+    def side_block(s, long):
+        block = jnp.where(lower == long, sp + away(s), sp - away(s))
+
+        @pl.when((block >= 0) & (block < n_sp) & (block != last))
+        def _():
+            with scope("absorb"):
+                absorb_all(block)
 
     @pl.loop(1, n_sp)
     def _(s):
-        with scope("fwd"):
-            forward(s)
-
-        @pl.loop(0, 2)
-        def _(way):
-            block = sp + s * (2 * way - 1)
-
-            @pl.when((block >= 0) & (block < n_sp) & (block != last))
-            def _():
-                with scope("absorb"):
-                    absorb_all(block)
+        side_block(s, True)
+
+        @pl.when(s + 1 < n_sp)
+        def _():
+            with scope("fwd"):
+                forward(s + 1)
+        side_block(s, False)
 
     if n_sp > 1:
         with scope("prepare"):
@@ -427,11 +484,11 @@
         @pl.loop(0, n_sp)
         def _(b):
             for part in range(2):
-                @pl.when((b <= sp) & (sp + 1 < n_sp))
+                @pl.when((b <= sp) & passes(b, sp + 1) | (b == sp) & (sp == n_sp - 1) & (n_sp > 2))
                 def _():
                     kv_copy(b, sp, 0, part).wait_send()
 
-                @pl.when((b >= sp) & (sp > 0))
+                @pl.when((b >= sp) & passes(b, sp - 1) | (b == sp) & (sp == 0) & (n_sp > 2))
                 def _():
                     kv_copy(b, sp, 1, part).wait_send()
 
@@ -449,18 +506,20 @@
     heads = qcols // hd
     deep, cols = shift_weight.shape
     vmem = pl.BlockSpec(memory_space=pltpu.VMEM)
-    smem = pl.BlockSpec(memory_space=pltpu.SMEM)
     hbm = pl.BlockSpec(memory_space=pl.ANY)
     dma = pltpu.SemaphoreType.DMA
     most = max(rows, crows)
     mid = rows // 2
     lanes = 2 * hd
     scratch = [
+        pltpu.VMEM((1, deep), BF16), pltpu.VMEM((deep,), BF16), pltpu.VMEM((1, width), F32),
+        pltpu.VMEM((1, hd), F32), pltpu.VMEM((1, hd), F32), pltpu.SMEM((heads,), F32),
         pltpu.VMEM((3, deep, cols), BF16),
         pltpu.VMEM((rows, width), BF16),
         pltpu.VMEM((crows, width), BF16),
         pltpu.VMEM((width, qcols), BF16),
         pltpu.VMEM((lanes, width), BF16),
+        pltpu.VMEM((width, lanes), BF16),
         pltpu.VMEM((n_tp,) + output_weight.shape, BF16),
         pltpu.VMEM((n_sp, 8, cols // 2), F32),
         pltpu.VMEM((n_tp, 8, cols // 2), F32),
@@ -477,7 +536,7 @@
         pltpu.VMEM((rows, lanes), F32),
         pltpu.VMEM((rows, lanes), F32),
         pltpu.VMEM((rows, 1), F32),
-        dma((9,)), pltpu.SemaphoreType.REGULAR,
+        dma((15,)), pltpu.SemaphoreType.REGULAR,
         dma((n_sp,)), dma((n_sp,)), dma((n_tp,)), dma((n_tp,)),
         dma((n_sp,)), dma((n_sp,)), dma((n_tp,)), dma((n_tp,)),
         dma((2, 2, n_sp)), dma((2, n_sp)),
@@ -487,7 +546,7 @@
     return pl.pallas_call(
         functools.partial(kernel, sizes),
         out_shape=pltpu.VMEM(latent.shape, BF16),
-        in_specs=[vmem] * 5 + [smem] + [hbm] * 9,
+        in_specs=[hbm] * 15,
         out_specs=vmem,
         scratch_shapes=scratch,
         compiler_params=pltpu.CompilerParams(

time: 35.7 us -> 33.9 us (0.950)
  Pallas kernels: 34.5 us -> 32.7 us
    pallas_call x1, Pallas kernels: 34.5 us -> 32.7 us  [on_device(): pl.pallas_call(functools.partial(kernel, sizes), out_shape=pltpu.VMEM(lat...]
where the time goes in v2:
time: 33.9 us; the launch traced here: 33.7 us
  Pallas kernels  32.7 us (96%)
  local copies, waits for them, and re-layouts  0.97 us (3%)
    pallas_call x1, Pallas kernels, on_device(): pl.pallas_call(functools.partial(kernel, sizes), out_shape=pltpu.VMEM(lat...  32.7 us
    unnamed x1, local copies, waits for them, and re-layouts  0.97 us

profile of v2, /device:TPU:0, one launch (start us, length us, event | category | flops | bytes accessed | tf_op | source)
XLA Modules:
  0.0 33.7 jit_solution(16743685114333143900)
XLA Ops:
  0.0 32.7 %shard_map.145 = bf16[1,256,2048]{2,1,0:T(8,128)(2,1)S(1)} custom-call(bf16[1,512]{1,0:T(2,128)(2,1)} %condition_h.1, bf16[512]{0:T(512)(128)(2,1)} %code_h.1, f32[1,2048]{1,0:T(1,128)} %bitcast.7, f32[1,64]{1,0:T(1,128)} %bitcast.8, f32[1,64]{1,0:T(1,128)} %bitcast.9, f32[4]{0:T(128)} %bias_h.1, bf16[1,256,2048]{2,1,0:T(8,128)(2,1)} %latent.1, ...), custom_call_target="tpu_custom_call" | custom-call | tf_op jit(solution)/shard_map/pallas_call | solution.py:546
  32.7 1.0 %copy.17 = bf16[1,256,2048]{2,1,0:T(8,128)(2,1)} copy(bf16[1,256,2048]{2,1,0:T(8,128)(2,1)S(1)} %shard_map.145) | data formatting | bytes 2097152

commit v3 on v2

--- a/solution.py
+++ b/solution.py
@@ -42,9 +42,7 @@
     condition, code, gain_ref, q_gain, k_gain, bias_ref,
     modw, lat, ctx, wq_v, wkv, wkv_t, wbuf,
     vec_z, vec_t, gate_z, gate_t, normed, kvbuf, vals, q_s, m_s, acc, att, mixed, cos_s, sin_s, inv_s,
-    local, met,
-    z_send, z_recv, t_send, t_recv, gz_send, gz_recv, gt_send, gt_recv, kv_send, kv_recv,
-    w_send, w_recv, f_send, f_recv, a_send, a_recv,
+    local, met, sent, came, kv_send, kv_recv, w_recv, x_recv, f_recv, a_recv,
 ):
     n_sp, n_tp, n_dp = sizes
     sp, tp, dp = lax.axis_index("sp"), lax.axis_index("tp"), lax.axis_index("dp")
@@ -77,15 +75,25 @@
             greet(barrier, dp=dp + d)
 
     copies = {}
-    for number, (name, src, dst) in enumerate((
-        ("condition", condition_h, condition), ("code", code_h, code),
-        ("m0", shift_w, modw.at[0]), ("m1", scale_w, modw.at[1]), ("m2", gate_w, modw.at[2]),
-        ("ctx", context.at[0], ctx), ("gain", gain_h, gain_ref), ("wk", wk, wkv.at[:hd]), ("wv", wv, wkv.at[hd:]),
-        ("k_gain", k_gain_h, k_gain), ("lat", latent.at[0], lat), ("q_gain", q_gain_h, q_gain), ("bias", bias_h, bias_ref),
-        ("wq", wq, wq_v), ("wo", wo, wbuf.at[tp]),
-    )):
+
+    def load(number, name, src, dst):
         copies[name] = pltpu.make_async_copy(src, dst, local.at[number])
         copies[name].start()
+
+    load(0, "condition", condition_h, condition)
+    load(1, "code", code_h, code)
+    load(2, "m0", shift_w, modw.at[0])
+    load(3, "m1", scale_w, modw.at[1])
+    load(4, "m2", gate_w, modw.at[2])
+    load(5, "ctx", context.at[0], ctx)
+    load(6, "gain", gain_h, gain_ref)
+    load(7, "wk", wk, wkv.at[:hd])
+    load(7, "wv", wv, wkv.at[hd:])
+    load(8, "lat", latent.at[0], lat)
+    load(9, "k_gain", k_gain_h, k_gain)
+
+    def drain(ref, sem):
+        pltpu.make_async_copy(ref, ref, sem).wait()
 
     def remote(src, dst, s, r, **where):
         return pltpu.make_async_remote_copy(
@@ -107,14 +115,16 @@
         rows4 = jnp.concatenate(pieces, axis=0)
         vec_z[sp] = jnp.concatenate([rows4[:, :side], rows4[:, side:]], axis=0)
 
+    load(0, "q_gain", q_gain_h, q_gain)
+    load(1, "bias", bias_h, bias_ref)
+    load(2, "wq", wq, wq_v)
+    load(3, "wo", wo, wbuf.at[tp])
+
     with scope("barrier"):
         pl.semaphore_wait(barrier, n_sp + n_tp - 2 + dp)
 
-    z_copies = []
     for d in range(1, n_sp):
-        copy = remote(vec_z.at[sp], vec_z.at[sp], z_send.at[d], z_recv.at[d], sp=(sp + d) % n_sp)
-        copy.start()
-        z_copies.append(copy)
+        remote(vec_z.at[sp], vec_z.at[sp], sent.at[0], came.at[0], sp=(sp + d) % n_sp).start()
     for d in range(1, n_dp):
         @pl.when(dp - d >= 0)
         def _():
@@ -123,31 +133,32 @@
     share = wo.shape[0] // n_dp
     piece = share // PARTS
     near = [d for d in (1, 2) if d < n_tp]
-    turns = {1: (2, 3, 0, 1), 2: (0, 1, 2, 3)}
-    waiting = []
-
-    def span(core, part):
-        return pl.ds(core * share + part * piece, piece)
+    turns = {1: ((2, 1), (3, 1), (0, 2)), 2: ((0, 1), (1, 1), (2, 2))}
+
+    def span(core, first, count):
+        return pl.ds(core * share + first * piece, count * piece)
 
     def send_weights(turn):
         for d in near:
-            part = turns[d][turn]
-            copy = remote(wo.at[span(dp, part)], wbuf.at[tp, span(dp, part)],
-                          w_send.at[d, part], w_recv.at[d, part], tp=tp ^ d)
-            copy.start()
-            waiting.append(copy)
-
-    def got_weights(d, part):
-        ref = wbuf.at[tp ^ d, span(dp, part)]
-        remote(ref, ref, w_send.at[d, part], w_recv.at[d, part], tp=tp ^ d).wait_recv()
-        if n_tp == 4 and d < 3 and part in turns[d][:2]:
-            copy = remote(ref, ref, w_send.at[3, part], w_recv.at[3, part], tp=tp ^ (3 - d))
-            copy.start()
-            waiting.append(copy)
+            area = span(dp, *turns[d][turn])
+            remote(wo.at[area], wbuf.at[tp, area], sent.at[4], w_recv.at[d - 1, turn], tp=tp ^ d).start()
+
+    def share_weights(ref):
         for e in range(1, n_dp):
-            copy = remote(ref, ref, f_send.at[d, part, e], f_recv.at[d, part, e], dp=(dp + e) % n_dp)
-            copy.start()
-            waiting.append(copy)
+            remote(ref, ref, sent.at[5], f_recv.at[e - 1], dp=(dp + e) % n_dp).start()
+
+    def got_weights(d, turn):
+        ref = wbuf.at[tp ^ d, span(dp, *turns[d][turn])]
+        drain(ref, w_recv.at[d - 1, turn])
+        if n_tp == 4 and turn < 2:
+            remote(ref, ref, sent.at[4], x_recv.at[d - 1], tp=tp ^ (3 - d)).start()
+        share_weights(ref)
+
+    def got_far():
+        for d in near:
+            ref = wbuf.at[tp ^ 3, span(dp, turns[d][0][0], 2)]
+            drain(ref, x_recv.at[d - 1])
+            share_weights(ref)
 
     send_weights(0)
 
@@ -155,11 +166,8 @@
         copies["m2"].wait()
         row = dots(both, modw[2])[:1]
         gate_z[sp] = jnp.concatenate([row[:, j * chip:(j + 1) * chip] for j in range(4)], axis=0)
-    g_copies = []
     for d in range(1, n_sp):
-        copy = remote(gate_z.at[sp], gate_z.at[sp], gz_send.at[d], gz_recv.at[d], sp=(sp + d) % n_sp)
-        copy.start()
-        g_copies.append(copy)
+        remote(gate_z.at[sp], gate_z.at[sp], sent.at[2], came.at[2], sp=(sp + d) % n_sp).start()
 
     with scope("tables"):
         cosine, sine = tables(sp * rows, rows, hd)
@@ -174,25 +182,22 @@
         inv_s[...] = lax.rsqrt(jnp.mean(floats * floats, axis=-1, keepdims=True) + norm_eps)
 
     with scope("turn"):
-        copies["wk"].wait()
-        copies["wv"].wait()
+        drain(wkv, local.at[7])
         wkv_t[...] = wkv[...].T
     with scope("zwait"):
-        for copy in z_copies:
-            copy.wait()
+        if n_sp > 1:
+            drain(vec_z.at[:n_sp - 1], came.at[0])
     total = vec_z[0]
     for k in range(1, n_sp):
         total = total + vec_z[k]
     vec_t[tp] = total
     for d in reversed(range(1, n_tp)):
-        copy = remote(vec_t.at[tp], vec_t.at[tp], t_send.at[d], t_recv.at[d], tp=tp ^ d)
-        copy.start()
-        waiting.append(copy)
-    for turn in range(1, PARTS):
+        remote(vec_t.at[tp], vec_t.at[tp], sent.at[1], came.at[1], tp=tp ^ d).start()
+    for turn in (1, 2):
         send_weights(turn)
     with scope("twait"):
-        for d in range(1, n_tp):
-            remote(vec_t.at[tp ^ d], vec_t.at[tp ^ d], t_send.at[d], t_recv.at[d], tp=tp ^ d).wait_recv()
+        if n_tp > 1:
+            drain(vec_t.at[:n_tp - 1], came.at[1])
 
     def modulate(tokens, inverse, which):
         for t in range(n_tp):
@@ -206,7 +211,7 @@
     def kv_copy(block, target, way, part):
         area = pl.ds(0, crows) if part == 0 else pl.ds(crows, rows)
         ref = kvbuf.at[block, area]
-        return remote(ref, ref, kv_send.at[way, part, block], kv_recv.at[part, block], sp=target)
+        return remote(ref, ref, kv_send.at[way, block], kv_recv.at[part, block], sp=target)
 
     def send_own(part):
         @pl.when(sp + 1 < n_sp)
@@ -268,7 +273,7 @@
             def _():
                 pl.semaphore_wait(met, 1)
         for d in near:
-            got_weights(d, turns[d][0])
+            got_weights(d, 0)
 
     with scope("qproj"):
         copies["wq"].wait()
@@ -287,16 +292,14 @@
                     q_s[half, h * mid:(h + 1) * mid] = one[half * mid:(half + 1) * mid]
 
     with scope("gatez"):
-        for copy in g_copies:
-            copy.wait()
+        if n_sp > 1:
+            drain(gate_z.at[:n_sp - 1], came.at[2])
         total = gate_z[0]
         for k in range(1, n_sp):
             total = total + gate_z[k]
         gate_t[tp] = total
     for d in range(1, n_tp):
-        copy = remote(gate_t.at[tp], gate_t.at[tp], gt_send.at[d], gt_recv.at[d], tp=tp ^ d)
-        copy.start()
-        waiting.append(copy)
+        remote(gate_t.at[tp], gate_t.at[tp], sent.at[3], came.at[3], tp=tp ^ d).start()
 
     def spread(column, count):
         if count % LANES == 0:
@@ -395,7 +398,7 @@
             forward(1, (1,))
     with scope("gotw1"):
         for d in near:
-            got_weights(d, turns[d][1])
+            got_weights(d, 1)
 
     def side_block(s, long):
         block = jnp.where(lower == long, sp + away(s), sp - away(s))
@@ -415,6 +418,9 @@
                 forward(s + 1)
         side_block(s, False)
 
+    with scope("gotw2"):
+        for d in near:
+            got_weights(d, 2)
     if n_sp > 1:
         with scope("prepare"):
             prepare(last)
@@ -429,14 +435,8 @@
             low = jnp.where(lane < hd, even, pltpu.roll(odd, hd, 1))
             att[tp, half, :, g * lanes:(g + 1) * lanes] = (top / low).astype(BF16)
         for d in reversed(range(1, n_tp)):
-            copy = remote(att.at[tp, half], att.at[tp, half], a_send.at[d, half], a_recv.at[d, half], tp=tp ^ d)
-            copy.start()
-            waiting.append(copy)
-
-    with scope("gotw2"):
-        for d in near:
-            for part in turns[d][2:]:
-                got_weights(d, part)
+            remote(att.at[tp, half], att.at[tp, half], sent.at[6], a_recv.at[half * d], tp=tp ^ d).start()
+
     copies["wo"].wait()
 
     def project(group, half, part):
@@ -451,22 +451,21 @@
 
     with scope("gotw3"):
         if n_tp == 4:
-            for part in range(PARTS):
-                got_weights(3, part)
-        for d in range(1, n_tp):
-            for core in range(1, n_dp):
-                source = (dp + n_dp - core) % n_dp
-                for part in range(PARTS):
-                    ref = wbuf.at[tp ^ d, span(source, part)]
-                    remote(ref, ref, f_send.at[d, part, core], f_recv.at[d, part, core], dp=source).wait_recv()
-            remote(gate_t.at[tp ^ d], gate_t.at[tp ^ d], gt_send.at[d], gt_recv.at[d], tp=tp ^ d).wait_recv()
+            got_far()
+        for e in range(1, n_dp):
+            if n_tp > 1:
+                drain(wbuf.at[:n_tp - 1, :share], f_recv.at[e - 1])
+        if n_tp > 1:
+            drain(gate_t.at[:n_tp - 1], came.at[3])
 
     order = [d for d in (2, 3, 1) if d < n_tp]
     for half in range(2):
         for d in order:
             with scope(f"att{half}{d}"):
-                ref = att.at[tp ^ d, half]
-                remote(ref, ref, a_send.at[d, half], a_recv.at[d, half], tp=tp ^ d).wait_recv()
+                if half == 0 and d == order[0]:
+                    drain(att.at[:n_tp - 1, 0], a_recv.at[0])
+                if half == 1:
+                    drain(att.at[tp ^ d, 1], a_recv.at[d])
             if d != order[-1]:
                 for part in parts:
                     mixed[tall[half], part] = mixed[tall[half], part] + project(tp ^ d, half, part)
@@ -478,19 +477,26 @@
             out[0, tall[half], part] = (lat[tall[half], part].astype(F32) + gate * value).astype(BF16)
 
     with scope("sendwait"):
-        for copy in waiting:
-            copy.wait_send()
+        if n_sp > 1:
+            drain(vec_z.at[:n_sp - 1], sent.at[0])
+            drain(gate_z.at[:n_sp - 1], sent.at[2])
+        if n_tp > 1:
+            drain(vec_t.at[:n_tp - 1], sent.at[1])
+            drain(gate_t.at[:n_tp - 1], sent.at[3])
+            drain(wbuf.at[:n_tp - 1, :share], sent.at[4])
+            for e in range(1, n_dp):
+                drain(wbuf.at[:n_tp - 1, :share], sent.at[5])
+            drain(att.at[:n_tp - 1], sent.at[6])
 
         @pl.loop(0, n_sp)
         def _(b):
-            for part in range(2):
-                @pl.when((b <= sp) & passes(b, sp + 1) | (b == sp) & (sp == n_sp - 1) & (n_sp > 2))
-                def _():
-                    kv_copy(b, sp, 0, part).wait_send()
-
-                @pl.when((b >= sp) & passes(b, sp - 1) | (b == sp) & (sp == 0) & (n_sp > 2))
-                def _():
-                    kv_copy(b, sp, 1, part).wait_send()
+            @pl.when((b <= sp) & passes(b, sp + 1) | (b == sp) & (sp == n_sp - 1) & (n_sp > 2))
+            def _():
+                drain(kvbuf.at[b], kv_send.at[0, b])
+
+            @pl.when((b >= sp) & passes(b, sp - 1) | (b == sp) & (sp == 0) & (n_sp > 2))
+            def _():
+                drain(kvbuf.at[b], kv_send.at[1, b])
 
 
 def on_device(
@@ -536,12 +542,8 @@
         pltpu.VMEM((rows, lanes), F32),
         pltpu.VMEM((rows, lanes), F32),
         pltpu.VMEM((rows, 1), F32),
-        dma((15,)), pltpu.SemaphoreType.REGULAR,
-        dma((n_sp,)), dma((n_sp,)), dma((n_tp,)), dma((n_tp,)),
-        dma((n_sp,)), dma((n_sp,)), dma((n_tp,)), dma((n_tp,)),
-        dma((2, 2, n_sp)), dma((2, n_sp)),
-        dma((n_tp, PARTS)), dma((n_tp, PARTS)), dma((n_tp, PARTS, n_dp)), dma((n_tp, PARTS, n_dp)),
-        dma((n_tp, 2)), dma((n_tp, 2)),
+        dma((10,)), pltpu.SemaphoreType.REGULAR, dma((7,)), dma((4,)),
+        dma((2, n_sp)), dma((2, n_sp)), dma((2, 3)), dma((2,)), dma((n_dp,)), dma((n_tp,)),
     ]
     return pl.pallas_call(
         functools.partial(kernel, sizes),

time: 33.9 us -> 32.6 us (0.962)
  Pallas kernels: 32.7 us -> 31.5 us
    pallas_call x1, Pallas kernels: 32.7 us -> 31.5 us  [on_device(): pl.pallas_call(functools.partial(kernel, sizes), out_shape=pltpu.VMEM(lat...]
where the time goes in v3:
time: 32.6 us; the launch traced here: 32.5 us
  Pallas kernels  31.5 us (97%)
  local copies, waits for them, and re-layouts  0.97 us (3%)
    pallas_call x1, Pallas kernels, on_device(): pl.pallas_call(functools.partial(kernel, sizes), out_shape=pltpu.VMEM(lat...  31.5 us
    unnamed x1, local copies, waits for them, and re-layouts  0.97 us

profile of v3, /device:TPU:0, one launch (start us, length us, event | category | flops | bytes accessed | tf_op | source)
XLA Modules:
  0.0 32.5 jit_solution(12318144425688479412)
XLA Ops:
  0.0 31.5 %shard_map.145 = bf16[1,256,2048]{2,1,0:T(8,128)(2,1)S(1)} custom-call(bf16[1,512]{1,0:T(2,128)(2,1)} %condition_h.1, bf16[512]{0:T(512)(128)(2,1)} %code_h.1, f32[1,2048]{1,0:T(1,128)} %bitcast.7, f32[1,64]{1,0:T(1,128)} %bitcast.8, f32[1,64]{1,0:T(1,128)} %bitcast.9, f32[4]{0:T(128)} %bias_h.1, bf16[1,256,2048]{2,1,0:T(8,128)(2,1)} %latent.1, ...), custom_call_target="tpu_custom_call" | custom-call | tf_op jit(solution)/shard_map/pallas_call | solution.py:548
  31.5 1.0 %copy.17 = bf16[1,256,2048]{2,1,0:T(8,128)(2,1)} copy(bf16[1,256,2048]{2,1,0:T(8,128)(2,1)S(1)} %shard_map.145) | data formatting | bytes 2097152

commit v4 on v3

--- a/solution.py
+++ b/solution.py
@@ -15,7 +15,6 @@
 BF16 = jnp.bfloat16
 LANES = 128
 LOG2E = math.log2(math.e)
-PARTS = 4
 GROUP = 2
 SCOPED_KIB = 64384
 
@@ -41,8 +40,8 @@
     out,
     condition, code, gain_ref, q_gain, k_gain, bias_ref,
     modw, lat, ctx, wq_v, wkv, wkv_t, wbuf,
-    vec_z, vec_t, gate_z, gate_t, normed, kvbuf, vals, q_s, m_s, acc, att, mixed, cos_s, sin_s, inv_s,
-    local, met, sent, came, kv_send, kv_recv, w_recv, x_recv, f_recv, a_recv,
+    vec_z, vec_t, gate_z, gate_t, normed_c, normed_l, kvbuf, vals, q_s, m_s, acc, att, mixed, cos_s, sin_s, inv_s,
+    local, met, sent, came, kv_send, kv_recv, w_recv, x_recv, s_recv, f_recv, a_recv,
 ):
     n_sp, n_tp, n_dp = sizes
     sp, tp, dp = lax.axis_index("sp"), lax.axis_index("tp"), lax.axis_index("dp")
@@ -86,11 +85,9 @@
     load(3, "m1", scale_w, modw.at[1])
     load(4, "m2", gate_w, modw.at[2])
     load(5, "ctx", context.at[0], ctx)
-    load(6, "gain", gain_h, gain_ref)
-    load(7, "wk", wk, wkv.at[:hd])
-    load(7, "wv", wv, wkv.at[hd:])
-    load(8, "lat", latent.at[0], lat)
-    load(9, "k_gain", k_gain_h, k_gain)
+    load(6, "wk", wk, wkv.at[:hd])
+    load(6, "wv", wv, wkv.at[hd:])
+    load(7, "lat", latent.at[0], lat)
 
     def drain(ref, sem):
         pltpu.make_async_copy(ref, ref, sem).wait()
@@ -115,8 +112,8 @@
         rows4 = jnp.concatenate(pieces, axis=0)
         vec_z[sp] = jnp.concatenate([rows4[:, :side], rows4[:, side:]], axis=0)
 
-    load(0, "q_gain", q_gain_h, q_gain)
-    load(1, "bias", bias_h, bias_ref)
+    load(0, "gain", gain_h, gain_ref)
+    load(1, "k_gain", k_gain_h, k_gain)
     load(2, "wq", wq, wq_v)
     load(3, "wo", wo, wbuf.at[tp])
 
@@ -131,17 +128,22 @@
             greet(met, dp=dp - d)
 
     share = wo.shape[0] // n_dp
-    piece = share // PARTS
+    piece = share // 8
     near = [d for d in (1, 2) if d < n_tp]
-    turns = {1: ((2, 1), (3, 1), (0, 2)), 2: ((0, 1), (1, 1), (2, 2))}
+    paired = n_sp % 2 == 0
+    turns = {1: ((3, 1), (4, 2), (0, 3)), 2: ((0, 1), (1, 2), (3, 3))}
 
     def span(core, first, count):
-        return pl.ds(core * share + first * piece, count * piece)
-
-    def send_weights(turn):
-        for d in near:
-            area = span(dp, *turns[d][turn])
-            remote(wo.at[area], wbuf.at[tp, area], sent.at[4], w_recv.at[d - 1, turn], tp=tp ^ d).start()
+        return pl.ds(pl.multiple_of(core * share + first * piece, piece), count * piece)
+
+    def extra(core, plane):
+        if paired:
+            return span(core, 6 + plane % 2, 1)
+        return span(core, 6, 2)
+
+    def send_weights(d, turn):
+        area = extra(dp, sp) if turn == 3 else span(dp, *turns[d][turn])
+        remote(wo.at[area], wbuf.at[tp, area], sent.at[4], w_recv.at[d - 1, turn], tp=tp ^ d).start()
 
     def share_weights(ref):
         for e in range(1, n_dp):
@@ -154,13 +156,48 @@
             remote(ref, ref, sent.at[4], x_recv.at[d - 1], tp=tp ^ (3 - d)).start()
         share_weights(ref)
 
+    def across(d):
+        ref = wbuf.at[tp ^ d, extra(dp, sp)]
+        if paired:
+            remote(ref, ref, sent.at[4], s_recv.at[d // 3], sp=sp ^ 1).start()
+
+    def got_extra():
+        for d in near:
+            ref = wbuf.at[tp ^ d, extra(dp, sp)]
+            drain(ref, w_recv.at[d - 1, 3])
+            if n_tp == 4:
+                @pl.when(dp % 2 == 2 - d)
+                def _():
+                    remote(ref, ref, sent.at[4], x_recv.at[2], tp=tp ^ (3 - d)).start()
+            across(d)
+
+    def share_extra():
+        for d in near:
+            share_weights(wbuf.at[tp ^ d, extra(dp, sp)])
+
+    def got_extra_far():
+        ref = wbuf.at[tp ^ 3, extra(dp, sp)]
+        drain(ref, x_recv.at[2])
+        across(3)
+        share_weights(ref)
+
+    def got_across(far):
+        if paired:
+            area = extra(dp, sp + 1)
+            those = [3] if far else near
+            drain(wbuf.at[:len(those), area], s_recv.at[1 if far else 0])
+            for d in those:
+                share_weights(wbuf.at[tp ^ d, area])
+
     def got_far():
         for d in near:
-            ref = wbuf.at[tp ^ 3, span(dp, turns[d][0][0], 2)]
+            ref = wbuf.at[tp ^ 3, span(dp, turns[d][0][0], 3)]
             drain(ref, x_recv.at[d - 1])
             share_weights(ref)
 
-    send_weights(0)
+    for turn in (3, 0):
+        for d in near:
+            send_weights(d, turn)
 
     with scope("gate"):
         copies["m2"].wait()
@@ -182,8 +219,9 @@
         inv_s[...] = lax.rsqrt(jnp.mean(floats * floats, axis=-1, keepdims=True) + norm_eps)
 
     with scope("turn"):
-        drain(wkv, local.at[7])
-        wkv_t[...] = wkv[...].T
+        drain(wkv, local.at[6])
+        for d in range(n_tp):
+            wkv_t[d * cols:(d + 1) * cols] = wkv[:, pl.ds(pl.multiple_of((tp ^ d) * cols, cols), cols)].T
     with scope("zwait"):
         if n_sp > 1:
             drain(vec_z.at[:n_sp - 1], came.at[0])
@@ -192,26 +230,30 @@
         total = total + vec_z[k]
     vec_t[tp] = total
     for d in reversed(range(1, n_tp)):
-        remote(vec_t.at[tp], vec_t.at[tp], sent.at[1], came.at[1], tp=tp ^ d).start()
+        remote(vec_t.at[tp], vec_t.at[tp], sent.at[1], came.at[1 if d in near else 4], tp=tp ^ d).start()
+    with scope("extra"):
+        got_extra()
     for turn in (1, 2):
-        send_weights(turn)
-    with scope("twait"):
-        if n_tp > 1:
-            drain(vec_t.at[:n_tp - 1], came.at[1])
-
-    def modulate(tokens, inverse, which):
-        for t in range(n_tp):
+        for d in near:
+            send_weights(d, turn)
+    early, far = [0] + near, list(range(3, n_tp))
+    cut = len(early) * cols
+
+    def modulate(tokens, inverse, which, normed, offsets):
+        for d in offsets:
+            t = tp ^ d
             for k in range(2):
-                part = slice(t * cols + k * side, t * cols + (k + 1) * side)
+                part = pl.ds(pl.multiple_of(t * cols + k * side, side), side)
                 at = 4 * k + which
                 factor = gain_ref[:, part] * (1.0 + vec_t[t, at + 2:at + 3, :])
                 shift = vec_t[t, at:at + 1, :]
-                normed[:tokens.shape[0], part] = (tokens[:, part].astype(F32) * inverse * factor + shift).astype(BF16)
+                values = tokens[:, part].astype(F32) * inverse * factor + shift
+                normed[:, d * cols + k * side:d * cols + (k + 1) * side] = values.astype(BF16)
 
     def kv_copy(block, target, way, part):
         area = pl.ds(0, crows) if part == 0 else pl.ds(crows, rows)
         ref = kvbuf.at[block, area]
-        return remote(ref, ref, kv_send.at[way, block], kv_recv.at[part, block], sp=target)
+        return remote(ref, ref, kv_send.at[0], kv_recv.at[part, block], sp=target)
 
     def send_own(part):
         @pl.when(sp + 1 < n_sp)
@@ -243,8 +285,7 @@
         lane = lax.broadcasted_iota(jnp.int32, values.shape, 1) % hd
         return jnp.where(lane < hd // 2, pltpu.roll(values, lanes - hd // 2, 1), pltpu.roll(values, hd // 2, 1))
 
-    def key_values(count, turn):
-        kv = dots(normed[:count], wkv_t[...])
+    def key_values(kv, turn):
         lane = lax.broadcasted_iota(jnp.int32, kv.shape, 1)
         keys = kv * lax.rsqrt(averages(kv) + norm_eps) * jnp.concatenate([k_gain[...]] * 2, axis=1)
         if turn:
@@ -252,18 +293,30 @@
         return jnp.where(lane < hd, keys, kv).astype(BF16)
 
     copies["gain"].wait()
+    copies["k_gain"].wait()
+    load(0, "q_gain", q_gain_h, q_gain)
+    load(1, "bias", bias_h, bias_ref)
+    with scope("twait1"):
+        if near:
+            drain(vec_t.at[:len(near)], came.at[1])
     with scope("modctx"):
-        modulate(ctx, inv_c, 1)
+        modulate(ctx, inv_c, 1, normed_c, early)
+        partial = dots(normed_c[:, :cut], wkv_t[:cut])
+        modulate(lat, inv_s[...], 0, normed_l, early)
+    with scope("twait2"):
+        for d in far:
+            drain(vec_t.at[tp ^ d], came.at[4])
     with scope("kvctx"):
-        copies["k_gain"].wait()
-        kvbuf[sp, :crows] = key_values(crows, False)
+        if far:
+            modulate(ctx, inv_c, 1, normed_c, far)
+            partial = partial + dots(normed_c[:, cut:], wkv_t[cut:])
+        kvbuf[sp, :crows] = key_values(partial, False)
     send_far(0)
     send_own(0)
 
-    with scope("modlat"):
-        modulate(lat, inv_s[...], 0)
     with scope("kvlat"):
-        kvbuf[sp, crows:] = key_values(rows, True)
+        modulate(lat, inv_s[...], 0, normed_l, far)
+        kvbuf[sp, crows:] = key_values(dots(normed_l[...], wkv_t[...]), True)
     send_far(1)
     send_own(1)
 
@@ -274,11 +327,14 @@
                 pl.semaphore_wait(met, 1)
         for d in near:
             got_weights(d, 0)
+        share_extra()
 
     with scope("qproj"):
         copies["wq"].wait()
         copies["q_gain"].wait()
-        queries = dots(normed[:rows], wq_v[...])
+        queries = functools.reduce(jnp.add, [
+            dots(normed_l[:, d * cols:(d + 1) * cols], wq_v[pl.ds(pl.multiple_of((tp ^ d) * cols, cols), cols)])
+            for d in range(n_tp)])
         factor = lax.rsqrt(averages(queries) + norm_eps)
         gains = jnp.concatenate([q_gain[...]] * 2, axis=1) * (hd ** -0.5 * LOG2E)
         lane = lax.broadcasted_iota(jnp.int32, (rows, lanes), 1)
@@ -388,6 +444,9 @@
     with scope("absorb0"):
         prepare(sp)
         absorb(sp, 0, True)
+    with scope("got1"):
+        for d in near:
+            got_weights(d, 1)
     if n_sp > 1:
         with scope("fwd1c"):
             forward(1, (0,))
@@ -396,10 +455,6 @@
     if n_sp > 1:
         with scope("fwd1l"):
             forward(1, (1,))
-    with scope("gotw1"):
-        for d in near:
-            got_weights(d, 1)
-
     def side_block(s, long):
         block = jnp.where(lower == long, sp + away(s), sp - away(s))
 
@@ -410,17 +465,24 @@
 
     @pl.loop(1, n_sp)
     def _(s):
+        def onward():
+            @pl.when(s + 1 < n_sp)
+            def _():
+                with scope("fwd"):
+                    forward(s + 1)
+
         side_block(s, True)
-
-        @pl.when(s + 1 < n_sp)
+        if n_sp > 4:
+            onward()
+        side_block(s, False)
+        if n_sp <= 4:
+            onward()
+
+    if n_tp == 4:
+        @pl.when(dp == 0)
         def _():
-            with scope("fwd"):
-                forward(s + 1)
-        side_block(s, False)
-
-    with scope("gotw2"):
-        for d in near:
-            got_weights(d, 2)
+            got_extra_far()
+
     if n_sp > 1:
         with scope("prepare"):
             prepare(last)
@@ -437,6 +499,15 @@
         for d in reversed(range(1, n_tp)):
             remote(att.at[tp, half], att.at[tp, half], sent.at[6], a_recv.at[half * d], tp=tp ^ d).start()
 
+    with scope("gotw1"):
+        if n_tp == 4:
+            @pl.when(dp > 0)
+            def _():
+                got_extra_far()
+        for d in near:
+            got_weights(d, 2)
+        if near:
+            got_across(False)
     copies["wo"].wait()
 
     def project(group, half, part):
@@ -452,13 +523,14 @@
     with scope("gotw3"):
         if n_tp == 4:
             got_far()
+            got_across(True)
         for e in range(1, n_dp):
             if n_tp > 1:
                 drain(wbuf.at[:n_tp - 1, :share], f_recv.at[e - 1])
         if n_tp > 1:
             drain(gate_t.at[:n_tp - 1], came.at[3])
 
-    order = [d for d in (2, 3, 1) if d < n_tp]
+    order = [d for d in (1, 3, 2) if d < n_tp]
     for half in range(2):
         for d in order:
             with scope(f"att{half}{d}"):
@@ -488,15 +560,21 @@
                 drain(wbuf.at[:n_tp - 1, :share], sent.at[5])
             drain(att.at[:n_tp - 1], sent.at[6])
 
-        @pl.loop(0, n_sp)
-        def _(b):
-            @pl.when((b <= sp) & passes(b, sp + 1) | (b == sp) & (sp == n_sp - 1) & (n_sp > 2))
-            def _():
-                drain(kvbuf.at[b], kv_send.at[0, b])
-
-            @pl.when((b >= sp) & passes(b, sp - 1) | (b == sp) & (sp == 0) & (n_sp > 2))
-            def _():
-                drain(kvbuf.at[b], kv_send.at[1, b])
+        if n_sp == 2:
+            drain(kvbuf.at[:1], kv_send.at[0])
+        if n_sp > 2:
+            fewer = (sp == 1).astype(jnp.int32) + (sp == n_sp - 2).astype(jnp.int32)
+
+            @pl.when(edge)
+            def _():
+                drain(kvbuf.at[:2], kv_send.at[0])
+
+            for less in range(3):
+                @pl.when(jnp.logical_not(edge) & (fewer == less))
+                def _():
+                    drain(kvbuf.at[:min(n_sp, n_sp + 1 - less)], kv_send.at[0])
+                    if less == 0:
+                        drain(kvbuf.at[:1], kv_send.at[0])
 
 
 def on_device(
@@ -514,7 +592,6 @@
     vmem = pl.BlockSpec(memory_space=pltpu.VMEM)
     hbm = pl.BlockSpec(memory_space=pl.ANY)
     dma = pltpu.SemaphoreType.DMA
-    most = max(rows, crows)
     mid = rows // 2
     lanes = 2 * hd
     scratch = [
@@ -531,7 +608,8 @@
         pltpu.VMEM((n_tp, 8, cols // 2), F32),
         pltpu.VMEM((n_sp, 4, cols // 4), F32),
         pltpu.VMEM((n_tp, 4, cols // 4), F32),
-        pltpu.VMEM((most, width), BF16),
+        pltpu.VMEM((crows, width), BF16),
+        pltpu.VMEM((rows, width), BF16),
         pltpu.VMEM((n_sp, crows + rows, lanes), BF16),
         pltpu.VMEM((crows + rows, lanes), BF16),
         pltpu.VMEM((2, heads * mid, lanes), BF16),
@@ -542,8 +620,8 @@
         pltpu.VMEM((rows, lanes), F32),
         pltpu.VMEM((rows, lanes), F32),
         pltpu.VMEM((rows, 1), F32),
-        dma((10,)), pltpu.SemaphoreType.REGULAR, dma((7,)), dma((4,)),
-        dma((2, n_sp)), dma((2, n_sp)), dma((2, 3)), dma((2,)), dma((n_dp,)), dma((n_tp,)),
+        dma((8,)), pltpu.SemaphoreType.REGULAR, dma((7,)), dma((5,)),
+        dma((1,)), dma((2, n_sp)), dma((2, 4)), dma((3,)), dma((2,)), dma((max(1, n_dp - 1),)), dma((n_tp,)),
     ]
     return pl.pallas_call(
         functools.partial(kernel, sizes),

time: 32.6 us -> 31.4 us (0.963)
  Pallas kernels: 31.5 us -> 30.2 us
    pallas_call x1, Pallas kernels: 31.5 us -> 30.2 us  [on_device(): pl.pallas_call(functools.partial(kernel, sizes), out_shape=pltpu.VMEM(lat...]
where the time goes in v4:
time: 31.4 us; the launch traced here: 31.2 us
  Pallas kernels  30.2 us (96%)
  local copies, waits for them, and re-layouts  0.97 us (3%)
    pallas_call x1, Pallas kernels, on_device(): pl.pallas_call(functools.partial(kernel, sizes), out_shape=pltpu.VMEM(lat...  30.2 us
    unnamed x1, local copies, waits for them, and re-layouts  0.97 us

profile of v4, /device:TPU:0, one launch (start us, length us, event | category | flops | bytes accessed | tf_op | source)
XLA Modules:
  0.0 31.2 jit_solution(17947906868801081970)
XLA Ops:
  0.0 30.2 %shard_map.145 = bf16[1,256,2048]{2,1,0:T(8,128)(2,1)S(1)} custom-call(bf16[1,512]{1,0:T(2,128)(2,1)} %condition_h.1, bf16[512]{0:T(512)(128)(2,1)} %code_h.1, f32[1,2048]{1,0:T(1,128)} %bitcast.7, f32[1,64]{1,0:T(1,128)} %bitcast.8, f32[1,64]{1,0:T(1,128)} %bitcast.9, f32[4]{0:T(128)} %bias_h.1, bf16[1,256,2048]{2,1,0:T(8,128)(2,1)} %latent.1, ...), custom_call_target="tpu_custom_call" | custom-call | tf_op jit(solution)/shard_map/pallas_call | solution.py:626
  30.2 1.0 %copy.17 = bf16[1,256,2048]{2,1,0:T(8,128)(2,1)} copy(bf16[1,256,2048]{2,1,0:T(8,128)(2,1)S(1)} %shard_map.145) | data formatting | bytes 2097152

commit v5 on v4

--- a/solution.py
+++ b/solution.py
@@ -486,6 +486,22 @@
     if n_sp > 1:
         with scope("prepare"):
             prepare(last)
+
+    def send_attended(piece, sem):
+        def send(d):
+            ref = att.at[tp, piece]
+            remote(ref, ref, sent.at[6], a_recv.at[sem * d], tp=tp ^ d).start()
+
+        if n_tp == 4:
+            send(2)
+            for flag, first in ((tp == 1, 1), (tp != 1, 3)):
+                @pl.when(flag)
+                def _():
+                    send(first)
+                    send(4 - first)
+        else:
+            for d in range(1, n_tp):
+                send(d)
     lane = lax.broadcasted_iota(jnp.int32, (mid, lanes), 1)
     for half in range(2):
         if n_sp > 1:
@@ -496,8 +512,7 @@
             top = jnp.where(lane < hd, pltpu.roll(even, hd, 1), odd)
             low = jnp.where(lane < hd, even, pltpu.roll(odd, hd, 1))
             att[tp, half, :, g * lanes:(g + 1) * lanes] = (top / low).astype(BF16)
-        for d in reversed(range(1, n_tp)):
-            remote(att.at[tp, half], att.at[tp, half], sent.at[6], a_recv.at[half * d], tp=tp ^ d).start()
+        send_attended(half, half)
 
     with scope("gotw1"):
         if n_tp == 4:

time: 31.4 us -> 30.9 us (0.984)
  Pallas kernels: 30.2 us -> 29.8 us
    pallas_call x1, Pallas kernels: 30.2 us -> 29.8 us  [on_device(): pl.pallas_call(functools.partial(kernel, sizes), out_shape=pltpu.VMEM(lat...]
where the time goes in v5:
time: 30.9 us; the launch traced here: 30.7 us
  Pallas kernels  29.8 us (96%)
  local copies, waits for them, and re-layouts  0.97 us (3%)
    pallas_call x1, Pallas kernels, on_device(): pl.pallas_call(functools.partial(kernel, sizes), out_shape=pltpu.VMEM(lat...  29.8 us
    unnamed x1, local copies, waits for them, and re-layouts  0.97 us

profile of v5, /device:TPU:0, one launch (start us, length us, event | category | flops | bytes accessed | tf_op | source)
XLA Modules:
  0.0 30.7 jit_solution(16172724136751117505)
XLA Ops:
  0.0 29.8 %shard_map.145 = bf16[1,256,2048]{2,1,0:T(8,128)(2,1)S(1)} custom-call(bf16[1,512]{1,0:T(2,128)(2,1)} %condition_h.1, bf16[512]{0:T(512)(128)(2,1)} %code_h.1, f32[1,2048]{1,0:T(1,128)} %bitcast.7, f32[1,64]{1,0:T(1,128)} %bitcast.8, f32[1,64]{1,0:T(1,128)} %bitcast.9, f32[4]{0:T(128)} %bias_h.1, bf16[1,256,2048]{2,1,0:T(8,128)(2,1)} %latent.1, ...), custom_call_target="tpu_custom_call" | custom-call | tf_op jit(solution)/shard_map/pallas_call | solution.py:641
  29.8 1.0 %copy.17 = bf16[1,256,2048]{2,1,0:T(8,128)(2,1)} copy(bf16[1,256,2048]{2,1,0:T(8,128)(2,1)S(1)} %shard_map.145) | data formatting | bytes 2097152

commit v6 on v5

--- a/solution.py
+++ b/solution.py
@@ -85,9 +85,6 @@
     load(3, "m1", scale_w, modw.at[1])
     load(4, "m2", gate_w, modw.at[2])
     load(5, "ctx", context.at[0], ctx)
-    load(6, "wk", wk, wkv.at[:hd])
-    load(6, "wv", wv, wkv.at[hd:])
-    load(7, "lat", latent.at[0], lat)
 
     def drain(ref, sem):
         pltpu.make_async_copy(ref, ref, sem).wait()
@@ -100,6 +97,9 @@
     with scope("modmat"):
         copies["condition"].wait()
         copies["code"].wait()
+        load(0, "lat", latent.at[0], lat)
+        load(1, "wk", wk, wkv.at[:hd])
+        load(1, "wv", wv, wkv.at[hd:])
         row8 = lax.broadcasted_iota(jnp.int32, (8, condition.shape[1]), 0)
         own_code = condition[...].astype(F32)
         shared_code = code[...].astype(F32)[None]
@@ -112,10 +112,8 @@
         rows4 = jnp.concatenate(pieces, axis=0)
         vec_z[sp] = jnp.concatenate([rows4[:, :side], rows4[:, side:]], axis=0)
 
-    load(0, "gain", gain_h, gain_ref)
-    load(1, "k_gain", k_gain_h, k_gain)
-    load(2, "wq", wq, wq_v)
-    load(3, "wo", wo, wbuf.at[tp])
+    load(2, "gain", gain_h, gain_ref)
+    load(3, "k_gain", k_gain_h, k_gain)
 
     with scope("barrier"):
         pl.semaphore_wait(barrier, n_sp + n_tp - 2 + dp)
@@ -153,7 +151,7 @@
         ref = wbuf.at[tp ^ d, span(dp, *turns[d][turn])]
         drain(ref, w_recv.at[d - 1, turn])
         if n_tp == 4 and turn < 2:
-            remote(ref, ref, sent.at[4], x_recv.at[d - 1], tp=tp ^ (3 - d)).start()
+            remote(ref, ref, sent.at[4], x_recv.at[0], tp=tp ^ (3 - d)).start()
         share_weights(ref)
 
     def across(d):
@@ -168,7 +166,7 @@
             if n_tp == 4:
                 @pl.when(dp % 2 == 2 - d)
                 def _():
-                    remote(ref, ref, sent.at[4], x_recv.at[2], tp=tp ^ (3 - d)).start()
+                    remote(ref, ref, sent.at[4], x_recv.at[1], tp=tp ^ (3 - d)).start()
             across(d)
 
     def share_extra():
@@ -177,7 +175,7 @@
 
     def got_extra_far():
         ref = wbuf.at[tp ^ 3, extra(dp, sp)]
-        drain(ref, x_recv.at[2])
+        drain(ref, x_recv.at[1])
         across(3)
         share_weights(ref)
 
@@ -190,10 +188,9 @@
                 share_weights(wbuf.at[tp ^ d, area])
 
     def got_far():
-        for d in near:
-            ref = wbuf.at[tp ^ 3, span(dp, turns[d][0][0], 3)]
-            drain(ref, x_recv.at[d - 1])
-            share_weights(ref)
+        ref = wbuf.at[tp ^ 3, span(dp, 0, 6)]
+        drain(ref, x_recv.at[0])
+        share_weights(ref)
 
     for turn in (3, 0):
         for d in near:
@@ -201,6 +198,7 @@
 
     with scope("gate"):
         copies["m2"].wait()
+        load(4, "wq", wq, wq_v)
         row = dots(both, modw[2])[:1]
         gate_z[sp] = jnp.concatenate([row[:, j * chip:(j + 1) * chip] for j in range(4)], axis=0)
     for d in range(1, n_sp):
@@ -212,6 +210,7 @@
         sin_s[...] = sine
     with scope("inv"):
         copies["ctx"].wait()
+        load(5, "wo", wo, wbuf.at[tp])
         floats = ctx[...].astype(F32)
         inv_c = lax.rsqrt(jnp.mean(floats * floats, axis=-1, keepdims=True) + norm_eps)
         copies["lat"].wait()
@@ -219,7 +218,7 @@
         inv_s[...] = lax.rsqrt(jnp.mean(floats * floats, axis=-1, keepdims=True) + norm_eps)
 
     with scope("turn"):
-        drain(wkv, local.at[6])
+        drain(wkv, local.at[1])
         for d in range(n_tp):
             wkv_t[d * cols:(d + 1) * cols] = wkv[:, pl.ds(pl.multiple_of((tp ^ d) * cols, cols), cols)].T
     with scope("zwait"):
@@ -253,7 +252,8 @@
     def kv_copy(block, target, way, part):
         area = pl.ds(0, crows) if part == 0 else pl.ds(crows, rows)
         ref = kvbuf.at[block, area]
-        return remote(ref, ref, kv_send.at[0], kv_recv.at[part, block], sp=target)
+        return remote(ref, ref, kv_send.at[0],
+                      kv_recv.at[part, lax.rem(block - target - 1 + 2 * n_sp, n_sp)], sp=target)
 
     def send_own(part):
         @pl.when(sp + 1 < n_sp)
@@ -294,8 +294,8 @@
 
     copies["gain"].wait()
     copies["k_gain"].wait()
-    load(0, "q_gain", q_gain_h, q_gain)
-    load(1, "bias", bias_h, bias_ref)
+    load(2, "q_gain", q_gain_h, q_gain)
+    load(3, "bias", bias_h, bias_ref)
     with scope("twait1"):
         if near:
             drain(vec_t.at[:len(near)], came.at[1])
@@ -635,8 +635,8 @@
         pltpu.VMEM((rows, lanes), F32),
         pltpu.VMEM((rows, lanes), F32),
         pltpu.VMEM((rows, 1), F32),
-        dma((8,)), pltpu.SemaphoreType.REGULAR, dma((7,)), dma((5,)),
-        dma((1,)), dma((2, n_sp)), dma((2, 4)), dma((3,)), dma((2,)), dma((max(1, n_dp - 1),)), dma((n_tp,)),
+        dma((6,)), pltpu.SemaphoreType.REGULAR, dma((7,)), dma((5,)),
+        dma((1,)), dma((2, max(1, n_sp - 1))), dma((2, 4)), dma((2,)), dma((2,)), dma((max(1, n_dp - 1),)), dma((n_tp,)),
     ]
     return pl.pallas_call(
         functools.partial(kernel, sizes),

time: 30.9 us -> 30.8 us (level)
  no operation moved by 1% of the time
where the time goes in v6:
time: 30.8 us; the launch traced here: 30.7 us
  Pallas kernels  29.7 us (96%)
  local copies, waits for them, and re-layouts  0.97 us (3%)
    pallas_call x1, Pallas kernels, on_device(): pl.pallas_call(functools.partial(kernel, sizes), out_shape=pltpu.VMEM(lat...  29.7 us
    unnamed x1, local copies, waits for them, and re-layouts  0.97 us

profile of v6, /device:TPU:0, one launch (start us, length us, event | category | flops | bytes accessed | tf_op | source)
XLA Modules:
  0.0 30.7 jit_solution(14870390274508624361)
XLA Ops:
  0.0 29.7 %shard_map.145 = bf16[1,256,2048]{2,1,0:T(8,128)(2,1)S(1)} custom-call(bf16[1,512]{1,0:T(2,128)(2,1)} %condition_h.1, bf16[512]{0:T(512)(128)(2,1)} %code_h.1, f32[1,2048]{1,0:T(1,128)} %bitcast.7, f32[1,64]{1,0:T(1,128)} %bitcast.8, f32[1,64]{1,0:T(1,128)} %bitcast.9, f32[4]{0:T(128)} %bias_h.1, bf16[1,256,2048]{2,1,0:T(8,128)(2,1)} %latent.1, ...), custom_call_target="tpu_custom_call" | custom-call | tf_op jit(solution)/shard_map/pallas_call | solution.py:641
  29.7 1.0 %copy.17 = bf16[1,256,2048]{2,1,0:T(8,128)(2,1)} copy(bf16[1,256,2048]{2,1,0:T(8,128)(2,1)S(1)} %shard_map.145) | data formatting | bytes 2097152
